TPU v7x, 32 devices: a whole 2x2x4 slice. The times are simulated.
32 devices in a mesh: sp: 8 (over z, x), tp: 4 (over y, core).
Axes of the slice: x: 2, y: 2, z: 4, core: 2. Of those that a mesh axis runs over, the one named last changes fastest.
Arguments:
- moe_input: bfloat16 [1024, 2048], P('sp'), may hold values from -6 to 6
- out_grad: bfloat16 [1024, 2048], P('sp'), may hold values from -6 to 6
- routes: int32 [1024, 2], P('sp'), may hold values from 0 to 7, all different within a row; in each aligned block of 128 rows (0 to 127, 128 to 255, ...) at most 40 rows name the same one
- route_weight: float32 [1024, 2], P('sp'), may hold values from 0.2 to 1.2
- w_gate: bfloat16 [8, 2048, 2048], P('sp', None, 'tp'), may hold values from -0.125 to 0.125
- w_up: bfloat16 [8, 2048, 2048], P('sp', None, 'tp'), may hold values from -0.125 to 0.125
- w_down: bfloat16 [8, 2048, 2048], P('sp', 'tp'), may hold values from -0.125 to 0.125
- w_out: bfloat16 [2048, 4096], P(None, 'tp'), may hold values from -0.09375 to 0.09375
- query_heads: bfloat16 [16, 1024, 128], P('tp', 'sp'), may hold values from -6 to 6
- key_heads: bfloat16 [16, 1024, 128], P('tp', 'sp'), may hold values from -6 to 6
- value_heads: bfloat16 [16, 1024, 256], P('tp', 'sp'), may hold values from -6 to 6
- log_decay: float32 [16, 1024], P('tp', 'sp'), may hold values from -0.6 to 0
- state_in: float32 [16, 8, 128, 256], P('tp', 'sp'), may hold values from -4 to 4
Outputs:
- gate_grad: bfloat16 [8, 2048, 2048], P('sp', None, 'tp')
- up_grad: bfloat16 [8, 2048, 2048], P('sp', None, 'tp')
- down_grad: bfloat16 [8, 2048, 2048], P('sp', 'tp')
- out_proj_grad: float32 [2048, 4096], P('sp', 'tp')
- query_gradient: bfloat16 [16, 1024, 128], P('tp', 'sp')
- key_grad: bfloat16 [16, 1024, 128], P('tp', 'sp')
- value_grad: bfloat16 [16, 1024, 256], P('tp', 'sp')
Inputs may be any that keep to these rules, and one draw needn't show every extreme that they name: `routes`: each row names 2 different experts; within each aligned block of 128 tokens no expert is named more than 40 times, and exactly 40 times for some expert in some blocks.
All inputs are finite; a program needn't handle non-finite values.
Results may differ from a plain program's by a relative error of at most 0.025.
Values may be sent and summed in bfloat16 or wider, within the bound.
A program may use at most 64 MiB of HBM per device.

v0:
```python
import jax
import jax.numpy as jnp
from jax import lax
from jax.sharding import PartitionSpec as P

BLOCK = 64


exact_precision = lax.Precision.HIGHEST


def entering(shard, axis, join, neutral):
    count = lax.axis_size(axis)
    place = lax.axis_index(axis)
    ahead = count - 1 - place
    gathered = jax.tree.map(
        lambda a, kind: lax.all_gather(a.astype(kind), axis), shard, (jnp.bfloat16, jnp.bfloat16)
    )
    state = jax.tree.map(lambda a, e: jnp.zeros_like(a) + jnp.asarray(e, a.dtype), shard, neutral)

    def one(lap, state):
        source = count - 1 - lap
        return join(
            state,
            jax.tree.map(
                lambda a, own: lax.dynamic_index_in_dim(a, source, 0, False).astype(own.dtype),
                gathered,
                shard,
            ),
        )

    return lax.fori_loop(0, ahead, one, state)


def silu_slope(gate_pre):
    sigmoid_v = jax.nn.sigmoid(gate_pre)
    return sigmoid_v * (1.0 + gate_pre * (1.0 - sigmoid_v))


def decay_table(log_sums):
    block_size = log_sums.shape[-1]
    token_positions = jnp.arange(block_size)
    lower_mask = (token_positions[:, None] >= token_positions[None, :])[None]
    log_diff = jnp.where(lower_mask, log_sums[:, :, None] - log_sums[:, None, :], 0.0)
    return jnp.where(lower_mask, jnp.exp(log_diff), 0.0)


def forward_block(forwarded_state, inputs):
    query_rows, rescaled_keys, value_rows, head_gradients, log_sums = inputs
    decay_mat = decay_table(log_sums)
    scores = (
        jnp.einsum("htk,hsk->hts", query_rows, rescaled_keys, precision=exact_precision) * decay_mat
    )
    leading_decay = jnp.exp(log_sums)[:, :, None]
    trailing_decay = jnp.exp(log_sums[:, -1:] - log_sums)[:, :, None]
    blended_heads = jnp.einsum("hts,hsv->htv", scores, value_rows, precision=exact_precision)
    blended_heads = blended_heads + jnp.einsum(
        "imj,iju->imu", query_rows * leading_decay, forwarded_state, precision=exact_precision
    )
    back_scores = (
        jnp.einsum("htv,hsv->hts", head_gradients, value_rows, precision=exact_precision)
        * decay_mat
    )
    query_gradient = jnp.einsum(
        "hts,hsk->htk", back_scores, rescaled_keys, precision=exact_precision
    )
    query_gradient = query_gradient + jnp.einsum(
        "fqg,fug->fqu", head_gradients * leading_decay, forwarded_state, precision=exact_precision
    )
    forwarded_state = jnp.exp(log_sums[:, -1])[:, None, None] * forwarded_state + jnp.einsum(
        "nbq,nbc->nqc", rescaled_keys * trailing_decay, value_rows, precision=exact_precision
    )
    return (forwarded_state, (blended_heads, query_gradient))


def reverse_block(forwarded_state, inputs):
    query_rows, rescaled_keys, value_rows, head_gradients, log_sums = inputs
    decay_mat = decay_table(log_sums)
    scores = (
        jnp.einsum("htk,hsk->hts", query_rows, rescaled_keys, precision=exact_precision) * decay_mat
    )
    back_scores = (
        jnp.einsum("htv,hsv->hts", head_gradients, value_rows, precision=exact_precision)
        * decay_mat
    )
    leading_decay = jnp.exp(log_sums)[:, :, None]
    trailing_decay = jnp.exp(log_sums[:, -1:] - log_sums)[:, :, None]
    key_portion = jnp.einsum("hts,htk->hsk", back_scores, query_rows, precision=exact_precision)
    key_portion = key_portion + jnp.einsum(
        "lbg,ljg->lbj", value_rows * trailing_decay, forwarded_state, precision=exact_precision
    )
    value_portion = jnp.einsum("hts,htv->hsv", scores, head_gradients, precision=exact_precision)
    value_portion = value_portion + jnp.einsum(
        "bea,baz->bez", rescaled_keys * trailing_decay, forwarded_state, precision=exact_precision
    )
    forwarded_state = jnp.exp(log_sums[:, -1])[:, None, None] * forwarded_state + jnp.einsum(
        "byj,byg->bjg", query_rows * leading_decay, head_gradients, precision=exact_precision
    )
    return (forwarded_state, (key_portion, value_portion))


def link_states(higher_part, lower_part):
    return (
        higher_part[0] * lower_part[0],
        lower_part[1] + lower_part[0][:, None, None] * higher_part[1],
    )


def expert_backward(rows_in, grad_in, w_gate, w_up, w_down):
    gate_pre = jnp.einsum("erd,edf->erf", rows_in, w_gate, preferred_element_type=jnp.float32)
    up_pre = jnp.einsum("erd,edf->erf", rows_in, w_up, preferred_element_type=jnp.float32)
    active = jax.nn.silu(gate_pre)
    hidden = (active * up_pre).astype(jnp.bfloat16)
    hidden_back = jnp.einsum("erd,efd->erf", grad_in, w_down, preferred_element_type=jnp.float32)
    down_part = jnp.einsum("erf,erd->efd", hidden, grad_in, preferred_element_type=jnp.float32)
    gate_back = (hidden_back * up_pre * silu_slope(gate_pre)).astype(jnp.bfloat16)
    up_back = (hidden_back * active).astype(jnp.bfloat16)
    gate_part = jnp.einsum("erd,erf->edf", rows_in, gate_back, preferred_element_type=jnp.float32)
    up_part = jnp.einsum("erd,erf->edf", rows_in, up_back, preferred_element_type=jnp.float32)
    partial_value = jnp.einsum(
        "erf,edf->erd", gate_back, w_gate, preferred_element_type=jnp.float32
    )
    partial_value = partial_value + jnp.einsum(
        "erf,edf->erd", up_back, w_up, preferred_element_type=jnp.float32
    )
    return (
        gate_part.astype(jnp.bfloat16),
        up_part.astype(jnp.bfloat16),
        down_part.astype(jnp.bfloat16),
        partial_value.astype(jnp.bfloat16),
    )


def body(
    moe_input,
    out_grad,
    routes,
    route_weight,
    w_gate,
    w_up,
    w_down,
    w_out,
    query_heads,
    key_heads,
    value_heads,
    log_decay,
    state_in,
):
    tok_rows, model_width = moe_input.shape
    picks = routes.shape[1]
    experts = w_gate.shape[0] * lax.axis_size("sp")
    capacity = 5 * tok_rows * picks // (4 * experts)
    route_ids = routes.reshape(-1)
    routed = route_ids.shape[0]
    onehot = (route_ids[:, None] == jnp.arange(experts, dtype=jnp.int32)[None, :]).astype(jnp.int32)
    slot_index = jnp.sum(jnp.cumsum(onehot, axis=0) * onehot, axis=1) - 1
    target = route_ids * capacity + slot_index
    source = (
        jnp.full((experts * capacity,), routed, jnp.int32)
        .at[target]
        .set(jnp.arange(routed, dtype=jnp.int32))
    )
    filled = source < routed
    picked = jnp.where(filled, source, 0)
    token_idx = picked // picks
    weight_slot = jnp.where(filled, route_weight.reshape(-1)[picked], 0.0)
    send_rows = jnp.where(filled[:, None], moe_input[token_idx], jnp.zeros((), jnp.bfloat16))
    send_rows = send_rows.reshape(experts, capacity, model_width)
    send_grad = (weight_slot[:, None] * out_grad[token_idx].astype(jnp.float32)).astype(
        jnp.bfloat16
    )
    send_grad = send_grad.reshape(experts, capacity, model_width)
    group_count = lax.axis_size("tp")
    slice_width = model_width // group_count
    rows_in, grad_in = (
        lax.all_to_all(send_rows, "sp", split_axis=0, concat_axis=1, tiled=True),
        lax.all_to_all(send_grad, "sp", split_axis=0, concat_axis=1, tiled=True),
    )
    gate_grad, up_grad, down_grad, partial_value = expert_backward(
        rows_in, grad_in, w_gate, w_up, w_down
    )
    local_rows = partial_value.shape[1]
    grouped = partial_value.reshape(partial_value.shape[0], local_rows, group_count, slice_width)
    spread_parts = lax.all_to_all(grouped, "tp", split_axis=2, concat_axis=2, tiled=True)
    feature_part = jnp.sum(spread_parts.astype(jnp.float32), axis=2).astype(jnp.bfloat16)
    returned_part = lax.all_to_all(feature_part, "sp", split_axis=1, concat_axis=0, tiled=True)
    returned = lax.all_gather(returned_part, "tp", axis=2, tiled=True)
    gathered = returned.reshape(experts * capacity, model_width)[target].reshape(
        tok_rows, picks, model_width
    )
    mixed_grad = (
        out_grad.astype(jnp.float32) + jnp.sum(gathered.astype(jnp.float32), axis=1)
    ).astype(jnp.bfloat16)
    head_count = query_heads.shape[0]
    key_size = key_heads.shape[-1]
    value_size = value_heads.shape[-1]
    head_grad = jnp.dot(mixed_grad, w_out, preferred_element_type=jnp.float32).astype(jnp.bfloat16)
    head_gradients = (
        head_grad.reshape(tok_rows, head_count, value_size).transpose(1, 0, 2).astype(jnp.float32)
    )
    query_rows = query_heads.astype(jnp.float32)
    rescaled_keys = key_heads.astype(jnp.float32) * key_size ** (-0.5)
    value_rows = value_heads.astype(jnp.float32)
    block_count = tok_rows // BLOCK

    def to_blocks(array):
        return array.reshape(head_count, block_count, BLOCK, array.shape[-1]).transpose(1, 0, 2, 3)

    def from_blocks(array):
        return array.transpose(1, 0, 2, 3).reshape(head_count, tok_rows, array.shape[-1])

    log_sums = jnp.cumsum(log_decay.reshape(head_count, block_count, BLOCK), axis=2).transpose(
        1, 0, 2
    )
    inputs = (
        to_blocks(query_rows),
        to_blocks(rescaled_keys),
        to_blocks(value_rows),
        to_blocks(head_gradients),
        log_sums,
    )
    _, (blended_heads, query_gradient) = lax.scan(forward_block, state_in[:, 0], inputs)
    running_total = jnp.cumsum(log_decay, axis=1)
    carried = jnp.einsum(
        "byj,byg->bjg",
        query_rows * jnp.exp(running_total)[:, :, None],
        head_gradients,
        precision=exact_precision,
    )
    span_keep = jnp.exp(running_total[:, -1])
    incoming = entering(
        (span_keep, carried), "sp", link_states, (jnp.ones_like(span_keep), jnp.zeros_like(carried))
    )[1]
    _, (key_grad, value_grad) = lax.scan(reverse_block, incoming, inputs, reverse=True)
    mixed_flat = (
        from_blocks(blended_heads)
        .astype(jnp.bfloat16)
        .transpose(1, 0, 2)
        .reshape(tok_rows, head_count * value_size)
    )
    out_proj_grad = lax.psum_scatter(
        lax.dot_general(
            mixed_grad, mixed_flat, (((0,), (0,)), ((), ())), preferred_element_type=jnp.float32
        ).astype(jnp.bfloat16),
        "sp",
        scatter_dimension=0,
        tiled=True,
    ).astype(jnp.float32)
    query_gradient = from_blocks(query_gradient).astype(jnp.bfloat16)
    key_grad = (from_blocks(key_grad) * key_size ** (-0.5)).astype(jnp.bfloat16)
    value_grad = from_blocks(value_grad).astype(jnp.bfloat16)
    return (gate_grad, up_grad, down_grad, out_proj_grad, query_gradient, key_grad, value_grad)


def solution(mesh):
    return jax.shard_map(
        body,
        mesh=mesh,
        in_specs=(
            P("sp", None),
            P("sp", None),
            P("sp", None),
            P("sp", None),
            P("sp", None, "tp"),
            P("sp", None, "tp"),
            P("sp", "tp", None),
            P(None, "tp"),
            P("tp", "sp", None),
            P("tp", "sp", None),
            P("tp", "sp", None),
            P("tp", "sp"),
            P("tp", "sp", None, None),
        ),
        out_specs=(
            P("sp", None, "tp"),
            P("sp", None, "tp"),
            P("sp", "tp", None),
            P("sp", "tp"),
            P("tp", "sp", None),
            P("tp", "sp", None),
            P("tp", "sp", None),
        ),
        check_vma=False,
    )
```

profile of v0, /device:TPU:0, one launch (start us, length us, event | category | flops | bytes accessed | tf_op | source)
XLA Modules:
  0.0 334.4 jit_solution(13286429424124512285)
XLA Ops:
  10.3 1.4 scatter_custom_fusion
  11.9 3.0 gather_fusion
  14.9 2.6 broadcast_select_fusion
  17.5 7.3 %all-to-all-start = ((bf16[8,40,2048]{2,1,0:T(8,128)(2,1)}), bf16[8,40,2048]{2,1,0:T(8,128)(2,1)}, u32[]{:S(2)}, u32[]{:S(2)}) async-start(bf16[8,40,2048]{2,1,0:T(8,128)(2,1)} %broadcast_select_fusion), calls=%async_computation | async-start | bytes 2621440 | tf_op jit(solution)/shard_map/all_to_all | solution.py:176
  24.8 3.0 gather_fusion.2
  28.1 2.5 gather_fusion.1
  30.6 2.7 fusion.70
  33.3 23.0 %all-to-all-done = bf16[8,40,2048]{2,1,0:T(8,128)(2,1)} async-done(((bf16[8,40,2048]{2,1,0:T(8,128)(2,1)}), bf16[8,40,2048]{2,1,0:T(8,128)(2,1)}, u32[]{:S(2)}, u32[]{:S(2)}) %all-to-all-start) | async-done | bytes 1310752 | tf_op jit(solution)/shard_map/all_to_all | solution.py:176
  56.3 4.3 %all-to-all-start.1 = ((bf16[8,40,2048]{2,1,0:T(8,128)(2,1)}), bf16[8,40,2048]{2,1,0:T(8,128)(2,1)}, u32[]{:S(2)}, u32[]{:S(2)}) async-start(bf16[8,40,2048]{2,1,0:T(8,128)(2,1)} %fusion.70), calls=%async_computation.1 | async-start | bytes 2621440 | tf_op jit(solution)/shard_map/all_to_all | solution.py:177
  60.6 2.3 fusion.73
  63.0 3.3 fusion.76
  66.2 25.3 %all-to-all-done.1 = bf16[8,40,2048]{2,1,0:T(8,128)(2,1)} async-done(((bf16[8,40,2048]{2,1,0:T(8,128)(2,1)}), bf16[8,40,2048]{2,1,0:T(8,128)(2,1)}, u32[]{:S(2)}, u32[]{:S(2)}) %all-to-all-start.1) | async-done | bytes 1310752 | tf_op jit(solution)/shard_map/all_to_all | solution.py:177
  91.6 3.2 multiply_convert_fusion.1
  96.6 1.9 fusion.69
  98.5 4.1 %reshape.353 = bf16[1,320,4,512]{3,2,1,0:T(4,128)(2,1)} reshape(bf16[320,2048]{1,0:T(8,128)(2,1)} %fusion.69) | data formatting | bytes 2621440 | tf_op jit(solution)/shard_map/reshape | solution.py:183
  102.6 1.6 copy.168
  104.2 20.4 %all_to_all.35 = bf16[1,320,4,512]{3,1,0,2:T(8,128)(2,1)} all-to-all(bf16[1,320,4,512]{3,1,0,2:T(8,128)(2,1)S(1)} %copy.168), channel_id=1, replica_groups=mesh['sp'=8,'tp'=4] {'tp'}, dimensions={2} | all-to-all | bytes 2621440 | tf_op jit(solution)/shard_map/all_to_all | solution.py:184
  124.6 2.3 reduce_sum.33
  126.9 1.5 copy.203
  128.9 3.4 %reduce.10 = bf16[320,512]{1,0:T(8,128)(2,1)} reduce(bf16[320,1,512]{2,1,0:T(2,128)(2,1)S(1)} %bitcast.257, bf16[]{:T(256)} %broadcast.193), dimensions={1}, to_apply=%bitcast.184.reduce_sub_computation | reduce | bytes 655362
  133.5 14.1 %all_to_all.36 = bf16[8,2,10240]{2,1,0:T(2,128)(2,1)} all-to-all(bf16[8,2,10240]{2,1,0:T(2,128)(2,1)S(1)} %reshape.425), channel_id=1, replica_groups=mesh['sp'=8,'tp'=4] {'sp'}, dimensions={0} | all-to-all | bytes 655360 | tf_op jit(solution)/shard_map/all_to_all | solution.py:186
  147.6 2.5 reshape.426
  155.7 11.0 %all-gather.5.cloned.1.call-done = bf16[8,40,2048]{2,1,0:T(8,128)(2,1)} async-done(((bf16[8,40,512]{2,1,0:T(8,128)(2,1)}), bf16[8,40,2048]{2,1,0:T(8,128)(2,1)}) %all-gather.5.cloned.1.call-update) | async-done | bytes 1310736 | tf_op jit(solution)/shard_map/all_gather | solution.py:187
  166.7 4.8 %gather_fusion.3 = bf16[256,2048]{1,0:T(8,128)(2,1)} fusion(bf16[320,2048]{1,0:T(8,128)(2,1)} %bitcast.254, s32[1024]{0:T(1024)S(1)} %pad_clamp_fusion), kind=kCustom, calls=%fused_computation.3 | custom fusion | bytes 2098176 | tf_op jit(solution)/shard_map/gather | solution.py:188
  171.5 3.3 reshape.365
  174.8 5.1 %reduce_sum.35 = f32[128,2048]{1,0:T(8,128)} reduce(f32[128,2,2048]{2,1,0:T(2,128)} %reshape.365, f32[]{:T(128)} %constant.152.clone.1), dimensions={1}, to_apply=%region_5.6 | reduce | flops 262144 | bytes 3145732 | tf_op jit(solution)/shard_map/reduce_sum | solution.py:192
  179.9 3.3 convolution_convert_fusion.5
  187.3 14.4 %while.46 = (s32[]{:T(128)}, f32[4,128,256]{2,1,0:T(8,128)S(1)}, bf16[2,4,64,256]{3,2,0,1:T(8,128)(2,1)}, bf16[2,4,64,128]{3,2,1,0:T(8,128)(2,1)}, f32[2,4,64]{2...) while((s32[]{:T(128)}, f32[4,128,256]{2,1,0:T(8,128)S(1)}, ...), condition=%wide.region_8.9_spmd, body=%wide.region_7.8_spmd.sunk | while | flops 453611776 | bytes 10858797 | solution.py:222
  187.3 1.3 convolution_multiply_fusion.8
  188.6 1.3 fusion.161
  190.0 2.0 fusion.162
  194.5 1.3 convolution_multiply_fusion.8
  195.9 1.3 fusion.161
  197.2 2.0 fusion.162
  202.8 4.5 %convolution_convert_fusion = bf16[2048,1024]{1,0:T(8,128)(2,1)} fusion(bf16[128,1024]{0,1:T(8,128)(2,1)S(1)} %bitcast.264, f32[128,2048]{1,0:T(8,128)} %reduce_sum.35, bf16[128,2048]{1,0:T(8,128)(2,1)S(1)} %copy-done.1), kind=kOutput, calls=%fused_computation.99 | convolution fusion | flops 539754496 | bytes 6029312 | tf_op jit(solution)/shard_map/dot_general | solution.py:242
  209.6 21.8 %all-reduce = bf16[32]{0:T(256)(128)(2,1)S(1)} all-reduce(bf16[32]{0:T(256)(128)(2,1)S(1)} %dynamic-update-slice), channel_id=3, replica_groups=mesh['sp'=8,'tp'=4] {'sp'}, use_global_device_ids=true, to_apply=%add | all-reduce | flops 32 | bytes 128
  231.5 4.0 %fusion.67 = bf16[1,2048,512]{2,1,0:T(8,128)(2,1)} fusion(bf16[320,2048]{1,0:T(8,128)(2,1)} %bitcast.21, bf16[320,512]{1,0:T(8,128)(2,1)S(1)} %copy-done.20), kind=kOutput, calls=%fused_computation.105 | convolution fusion | flops 672137216 | bytes 3735552 | tf_op jit(solution)/shard_map/erd,erf->edf/dot_general | solution.py:119
  235.5 4.0 %fusion.66 = bf16[1,2048,512]{2,1,0:T(8,128)(2,1)} fusion(bf16[320,2048]{1,0:T(8,128)(2,1)} %bitcast.21, bf16[320,512]{1,0:T(8,128)(2,1)S(1)} %copy-done.14), kind=kOutput, calls=%fused_computation.104 | convolution fusion | flops 672137216 | bytes 3735552 | tf_op jit(solution)/shard_map/erd,erf->edf/dot_general | solution.py:118
  239.5 4.0 %fusion.68 = bf16[1,512,2048]{2,1,0:T(8,128)(2,1)} fusion(bf16[320,2048]{1,0:T(8,128)(2,1)} %bitcast.23, f32[320,512]{1,0:T(8,128)S(1)} %copy-done.29, f32[320,512]{1,0:T(8,128)S(1)} %copy-done.28), kind=kOutput, calls=%fused_computation.106 | convolution fusion | flops 673120256 | bytes 4718592 | tf_op jit(solution)/shard_map/erf,erd->efd/dot_general | solution.py:115
  244.2 8.3 %while.47 = (s32[]{:T(128)}, f32[4,128,256]{2,1,0:T(8,128)S(1)}, s32[]{:T(128)}, bf16[8,4,128,256]{3,2,1,0:T(8,128)(2,1)}, bf16[8,4]{1,0:T(8,128)(2,1)S(1)}, /*index=5*/s32[]{:T(128)}, s32[]{:T(128)}, s32[]{:T(128)}, s32[]{:T(128)}) while((s32[]{:T(128)}, f32[4,128,256]{2,1,0:T(8,128)S(1)}, s32[]{:T(128)}, ...), condition=%wide.region_12.13_spmd, body=%wide.region_11.12_spmd.sunk | while | flops 393226 | bytes 1310907 | solution.py:32
  253.9 14.3 %while.48 = (s32[]{:T(128)}, f32[4,128,256]{2,1,0:T(8,128)S(1)}, f32[2,4,64,128]{3,2,1,0:T(8,128)}, bf16[2,4,64,256]{3,2,1,0:T(8,128)(2,1)}, f32[2,4,64]{2,1,0:T...) while((s32[]{:T(128)}, f32[4,128,256]{2,1,0:T(8,128)S(1)}, ...), condition=%wide.region_14.15_spmd, body=%wide.region_13.14_spmd.sunk | while | flops 453611776 | bytes 10859325 | solution.py:234
  254.0 1.3 convolution_multiply_fusion.11
  255.3 1.4 fusion.179
  261.2 1.3 convolution_multiply_fusion.11
  262.5 1.4 fusion.179
  269.9 1.7 copy.186
  271.6 54.1 %reduce-scatter.2.cloned.1.call-done = bf16[256,1024]{1,0:T(8,128)(2,1)} async-done(((bf16[2048,1024]{1,0:T(8,128)(2,1)}), bf16[256,1024]{1,0:T(8,128)(2,1)}) %reduce-scatter.2.cloned.1.call-update) | async-done | bytes 524304 | tf_op jit(solution)/shard_map/reduce_scatter | solution.py:241
  325.7 2.1 convert_element_type.182
  (193 shorter events, 44.8 us)
Async XLA Ops:
  7.2 53.4 %copy-start = (bf16[1,2048,512]{2,1,0:T(8,128)(2,1)S(1)}, bf16[1,2048,512]{2,1,0:T(8,128)(2,1)}, u32[]{:S(2)}) copy-start(bf16[1,2048,512]{2,1,0:T(8,128)(2,1)} %param.23) | copy-start | bytes 6291460
  7.2 4.7 %copy-start.2 = (bf16[128,2048]{1,0:T(8,128)(2,1)S(1)}, bf16[128,2048]{1,0:T(8,128)(2,1)}, u32[]{:S(2)}) copy-start(bf16[128,2048]{1,0:T(8,128)(2,1)} %param.19) | copy-start | bytes 1572868
  10.3 1.5 copy-start.23
  14.9 9.9 %copy-start.1 = (bf16[128,2048]{1,0:T(8,128)(2,1)S(1)}, bf16[128,2048]{1,0:T(8,128)(2,1)}, u32[]{:S(2)}) copy-start(bf16[128,2048]{1,0:T(8,128)(2,1)} %param.20) | copy-start | bytes 1572868
  17.5 38.8 %all-to-all-start = ((bf16[8,40,2048]{2,1,0:T(8,128)(2,1)}), bf16[8,40,2048]{2,1,0:T(8,128)(2,1)}, u32[]{:S(2)}, u32[]{:S(2)}) async-start(bf16[8,40,2048]{2,1,0:T(8,128)(2,1)} %broadcast_select_fusion), calls=%async_computation | async-start | bytes 2621440 | tf_op jit(solution)/shard_map/all_to_all | solution.py:176
  24.8 3.0 copy-start.25
  56.3 35.3 %all-to-all-start.1 = ((bf16[8,40,2048]{2,1,0:T(8,128)(2,1)}), bf16[8,40,2048]{2,1,0:T(8,128)(2,1)}, u32[]{:S(2)}, u32[]{:S(2)}) async-start(bf16[8,40,2048]{2,1,0:T(8,128)(2,1)} %fusion.70), calls=%async_computation.1 | async-start | bytes 2621440 | tf_op jit(solution)/shard_map/all_to_all | solution.py:177
  60.6 106.1 %all-gather.5.cloned.1.call-start = ((), (), s32[]{:S(2)}) async-start(), calls=%async_computation.5 | async-start | bytes 1638400 | tf_op jit(solution)/shard_map/all_gather | solution.py:187
  60.6 2.3 copy-start.9
  62.9 28.6 %copy-start.27 = (f32[320,512]{1,0:T(8,128)}, f32[320,512]{1,0:T(8,128)S(1)}, u32[]{:S(2)}) copy-start(f32[320,512]{1,0:T(8,128)S(1)} %fusion.73) | copy-start | bytes 1966084
  94.7 0.9 copy-start.13
  94.8 0.9 copy-start.19
  94.8 1.8 copy-start.10
  128.9 22.0 %copy-start.22 = (f32[4,128]{1,0:T(4,128)S(1)}, f32[4,128]{1,0:T(4,128)}, u32[]{:S(2)}) copy-start(f32[4,128]{1,0:T(4,128)} %param.30) | copy-start | bytes 6148
  147.6 5.6 %copy-start.21 = (bf16[4,128,128]{2,1,0:T(8,128)(2,1)S(1)}, bf16[4,128,128]{2,1,0:T(8,128)(2,1)}, u32[]{:S(2)}) copy-start(bf16[4,128,128]{2,1,0:T(8,128)(2,1)} %param.28) | copy-start | bytes 393220
  150.1 3.2 copy-start.15
  150.9 4.1 %copy-start.24 = (s32[256,1]{0,1:T(1,128)S(1)}, s32[256,1]{0,1:T(1,128)}, u32[]{:S(2)}) copy-start(s32[256,1]{0,1:T(1,128)} %copy-done.23) | copy-start | bytes 3076
  150.9 93.3 %all-gather.7.cloned.1.call-start = ((), (), s32[]{:S(2)}) async-start(), calls=%async_computation.7 | async-start | bytes 2359296 | tf_op jit(solution)/shard_map/all_gather | solution.py:17
  183.2 4.1 %copy-start.3 = (f32[4,1,128,256]{3,2,1,0:T(8,128)S(1)}, f32[4,1,128,256]{3,2,1,0:T(8,128)}, u32[]{:S(2)}) copy-start(f32[4,1,128,256]{3,2,1,0:T(8,128)} %param.31) | copy-start | bytes 1572868
  185.2 140.6 %reduce-scatter.2.cloned.1.call-start = ((), (), s32[]{:S(2)}) async-start(), calls=%async_computation.6 | async-start | bytes 4718592 | tf_op jit(solution)/shard_map/reduce_scatter | solution.py:241
  187.3 4.7 %copy-start.4 = (f32[2,4,64,256]{3,2,1,0:T(8,128)S(1)}, f32[2,4,64,256]{3,2,1,0:T(8,128)}, u32[]{:S(2)}) copy-start(f32[2,4,64,256]{3,2,1,0:T(8,128)} %get-tuple-element.662) | copy-start | bytes 1572868 | tf_op jit(solution)/shard_map/while
  187.3 4.7 %copy-start.6 = (f32[2,4,64,256]{3,2,1,0:T(8,128)S(1)}, f32[2,4,64,256]{3,2,1,0:T(8,128)}, u32[]{:S(2)}) copy-start(f32[2,4,64,256]{3,2,1,0:T(8,128)} %get-tuple-element.664) | copy-start | bytes 1572868 | tf_op jit(solution)/shard_map/while
  187.3 5.4 %copy-start.16 = (bf16[2,4,64,128]{3,2,1,0:T(8,128)(2,1)S(1)}, bf16[2,4,64,128]{3,2,1,0:T(8,128)(2,1)}, u32[]{:S(2)}) copy-start(bf16[2,4,64,128]{3,2,1,0:T(8,128)(2,1)} %get-tuple-element.649) | copy-start | bytes 393220 | tf_op jit(solution)/shard_map/while
  193.4 1.1 copy-start.17
  194.5 4.7 %copy-start.4 = (f32[2,4,64,256]{3,2,1,0:T(8,128)S(1)}, f32[2,4,64,256]{3,2,1,0:T(8,128)}, u32[]{:S(2)}) copy-start(f32[2,4,64,256]{3,2,1,0:T(8,128)} %get-tuple-element.662) | copy-start | bytes 1572868 | tf_op jit(solution)/shard_map/while
  194.5 4.7 %copy-start.6 = (f32[2,4,64,256]{3,2,1,0:T(8,128)S(1)}, f32[2,4,64,256]{3,2,1,0:T(8,128)}, u32[]{:S(2)}) copy-start(f32[2,4,64,256]{3,2,1,0:T(8,128)} %get-tuple-element.664) | copy-start | bytes 1572868 | tf_op jit(solution)/shard_map/while
  194.5 5.4 %copy-start.16 = (bf16[2,4,64,128]{3,2,1,0:T(8,128)(2,1)S(1)}, bf16[2,4,64,128]{3,2,1,0:T(8,128)(2,1)}, u32[]{:S(2)}) copy-start(bf16[2,4,64,128]{3,2,1,0:T(8,128)(2,1)} %get-tuple-element.649) | copy-start | bytes 393220 | tf_op jit(solution)/shard_map/while
  200.6 1.1 copy-start.17
  207.3 0.7 copy-start.26
  207.3 24.2 %copy-start.20 = (bf16[320,512]{1,0:T(8,128)(2,1)S(1)}, bf16[320,512]{1,0:T(8,128)(2,1)}, u32[]{:S(2)}) copy-start(bf16[320,512]{1,0:T(8,128)(2,1)} %copy-done.19) | copy-start | bytes 983044
  231.5 4.0 %copy-start.14 = (bf16[320,512]{1,0:T(8,128)(2,1)S(1)}, bf16[320,512]{1,0:T(8,128)(2,1)}, u32[]{:S(2)}) copy-start(bf16[320,512]{1,0:T(8,128)(2,1)} %copy-done.13) | copy-start | bytes 983044
  235.5 4.0 %copy-start.28 = (f32[320,512]{1,0:T(8,128)S(1)}, f32[320,512]{1,0:T(8,128)}, u32[]{:S(2)}) copy-start(f32[320,512]{1,0:T(8,128)} %copy-done.27) | copy-start | bytes 1966084
  235.5 4.0 %copy-start.29 = (f32[320,512]{1,0:T(8,128)S(1)}, f32[320,512]{1,0:T(8,128)}, u32[]{:S(2)}) copy-start(f32[320,512]{1,0:T(8,128)} %fusion.76) | copy-start | bytes 1966084
  239.5 4.0 %copy-start.18 = (bf16[2,4,64,128]{3,2,1,0:T(8,128)(2,1)S(1)}, bf16[2,4,64,128]{3,2,1,0:T(8,128)(2,1)}, u32[]{:S(2)}) copy-start(bf16[2,4,64,128]{3,2,1,0:T(8,128)(2,1)} %get-tuple-element.320) | copy-start | bytes 393220
  244.2 9.7 %copy-start.5 = (f32[2,4,64,256]{3,2,1,0:T(8,128)S(1)}, f32[2,4,64,256]{3,2,1,0:T(8,128)}, u32[]{:S(2)}) copy-start(f32[2,4,64,256]{3,2,1,0:T(8,128)} %get-tuple-element.726) | copy-start | bytes 1572868
  253.9 4.1 %copy-start.7 = (f32[2,4,64,256]{3,2,1,0:T(8,128)S(1)}, f32[2,4,64,256]{3,2,1,0:T(8,128)}, u32[]{:S(2)}) copy-start(f32[2,4,64,256]{3,2,1,0:T(8,128)} %get-tuple-element.719) | copy-start | bytes 1572868 | tf_op jit(solution)/shard_map/while
  253.9 4.5 %copy-start.8 = (f32[2,4,64,128]{3,2,1,0:T(8,128)S(1)}, f32[2,4,64,128]{3,2,1,0:T(8,128)}, u32[]{:S(2)}) copy-start(f32[2,4,64,128]{3,2,1,0:T(8,128)} %get-tuple-element.718) | copy-start | bytes 786436 | tf_op jit(solution)/shard_map/while
  253.9 4.9 %copy-start.11 = (f32[2,4,64,128]{3,2,1,0:T(8,128)S(1)}, f32[2,4,64,128]{3,2,1,0:T(8,128)}, u32[]{:S(2)}) copy-start(f32[2,4,64,128]{3,2,1,0:T(8,128)} %get-tuple-element.705) | copy-start | bytes 786436 | tf_op jit(solution)/shard_map/while
  259.6 0.7 copy-start.12
  261.1 4.2 %copy-start.7 = (f32[2,4,64,256]{3,2,1,0:T(8,128)S(1)}, f32[2,4,64,256]{3,2,1,0:T(8,128)}, u32[]{:S(2)}) copy-start(f32[2,4,64,256]{3,2,1,0:T(8,128)} %get-tuple-element.719) | copy-start | bytes 1572868 | tf_op jit(solution)/shard_map/while
  261.1 4.6 %copy-start.8 = (f32[2,4,64,128]{3,2,1,0:T(8,128)S(1)}, f32[2,4,64,128]{3,2,1,0:T(8,128)}, u32[]{:S(2)}) copy-start(f32[2,4,64,128]{3,2,1,0:T(8,128)} %get-tuple-element.718) | copy-start | bytes 786436 | tf_op jit(solution)/shard_map/while
  261.1 5.0 %copy-start.11 = (f32[2,4,64,128]{3,2,1,0:T(8,128)S(1)}, f32[2,4,64,128]{3,2,1,0:T(8,128)}, u32[]{:S(2)}) copy-start(f32[2,4,64,128]{3,2,1,0:T(8,128)} %get-tuple-element.705) | copy-start | bytes 786436 | tf_op jit(solution)/shard_map/while
  266.8 0.7 copy-start.12
Sparse Core Ops, SparseCore 0:
  151.0 15.5 all-gather.4
  185.3 49.9 all-gather.6
  238.9 86.7 reduce-scatter.1
where the time goes:
time: 336 us; the launch traced here: 334 us
  waiting for transfers between devices  113 us (34%)
  matrix products  58.2 us (17%)
  blocking collectives  56.3 us (17%)
  local copies, waits for them, and re-layouts  45.8 us (14%)
  other arithmetic  33.1 us (10%)
  between operations  14.8 us (4%)
  starting transfers between devices  11.9 us (4%)
    reduce_scatter x1, waiting for transfers between devices, body(): lax.psum_scatter(lax.dot_general(mixed_grad, mixed_flat, (((0,), (0,)), (...  54.1 us
    all_to_all x1, waiting for transfers between devices, body(): lax.all_to_all(send_grad, 'sp', split_axis=0, concat_axis=1, tiled=True)  25.3 us
    all_to_all x1, waiting for transfers between devices, body(): lax.all_to_all(send_rows, 'sp', split_axis=0, concat_axis=1, tiled=True)  23 us
    unnamed x1, blocking collectives  21.8 us
    all_to_all x1, blocking collectives, body(): lax.all_to_all(grouped, 'tp', split_axis=2, concat_axis=2, tiled=True)  20.4 us
    all_to_all x1, blocking collectives, body(): lax.all_to_all(feature_part, 'sp', split_axis=1, concat_axis=0, tiled=True)  14.1 us
    all_gather x1, waiting for transfers between devices, body(): returned = lax.all_gather(returned_part, 'tp', axis=2, tiled=True)  11 us
    unnamed x53, local copies, waits for them, and re-layouts  8.41 us
  transfers between devices with their start and end apart: 5, of which 4 were waited for; matrix products, arithmetic and copies ran while one was open for 24% of the time, Pallas kernels for 0%

commit v1 on v0

v1 whole, which is shorter than its diff:
```python
import jax
import jax.numpy as jnp
from jax import lax
from jax.sharding import PartitionSpec as P

F32 = jnp.float32
BF16 = jnp.bfloat16


def dot(spec, a, b):
    return jnp.einsum(spec, a, b, preferred_element_type=F32)


def dispatch_table(routes, route_weight, experts, capacity):
    tok_rows = routes.shape[0]
    named = routes[:, :, None] == jnp.arange(experts, dtype=jnp.int32)[None, None, :]
    member = jnp.any(named, axis=1)
    weight = jnp.sum(jnp.where(named, route_weight[:, :, None], 0.0), axis=1)
    spot = jnp.arange(tok_rows)
    earlier = (spot[:, None] > spot[None, :]).astype(BF16)
    rank = dot("ts,se->et", earlier, member.astype(BF16)).astype(jnp.int32)
    slots = jnp.arange(capacity, dtype=jnp.int32)
    table = (rank[:, None, :] == slots[None, :, None]) & member.T[:, None, :]
    slot_weight = jnp.sum(jnp.where(table, weight.T[:, None, :], 0.0), axis=2)
    return table.astype(BF16), slot_weight


def quarter(array, axis_name, axis):
    width = array.shape[axis] // lax.axis_size(axis_name)
    return lax.dynamic_slice_in_dim(array, lax.axis_index(axis_name) * width, width, axis)


def join_features(rows):
    gathered = lax.all_gather(rows, "tp", axis=0)
    return jnp.concatenate([gathered[i] for i in range(gathered.shape[0])], axis=1)


def exchange(array, axis, step):
    count = lax.axis_size(axis)
    return lax.ppermute(array, axis, [(i, i ^ step) for i in range(count)])


def sum_features(value):
    count = lax.axis_size("tp")
    place = lax.axis_index("tp")
    width = value.shape[1] // count
    parts = [value[:, i * width : (i + 1) * width] for i in range(count)]
    step = 1
    while len(parts) > 1:
        upper = (place // step) % 2 == 1
        keep = [jnp.where(upper, b, a) for a, b in zip(parts[::2], parts[1::2])]
        send = [jnp.where(upper, a, b).astype(BF16) for a, b in zip(parts[::2], parts[1::2])]
        got = exchange(jnp.stack(send), "tp", step)
        parts = [k.astype(F32) + got[i].astype(F32) for i, k in enumerate(keep)]
        step *= 2
    return parts[0].astype(BF16)


def silu_slope(gate_pre):
    sigmoid_v = jax.nn.sigmoid(gate_pre)
    return sigmoid_v * (1.0 + gate_pre * (1.0 - sigmoid_v))


def body(
    moe_input,
    out_grad,
    routes,
    route_weight,
    w_gate,
    w_up,
    w_down,
    w_out,
    query_heads,
    key_heads,
    value_heads,
    log_decay,
    state_in,
):
    tok_rows, model_width = moe_input.shape
    picks = routes.shape[1]
    spans = lax.axis_size("sp")
    place = lax.axis_index("sp")
    experts = w_gate.shape[0] * spans
    capacity = 5 * tok_rows * picks // (4 * experts)
    head_count, _, key_size = key_heads.shape
    value_size = value_heads.shape[-1]
    scale = key_size ** (-0.5)
    wg, wu, wd = w_gate[0], w_up[0], w_down[0]

    table, slot_weight = dispatch_table(routes, route_weight, experts, capacity)
    out_grad_q = quarter(out_grad, "tp", 1)
    send_rows = dot("ect,td->ecd", table, quarter(moe_input, "tp", 1)).astype(BF16)
    send_grad = (dot("ect,td->ecd", table, out_grad_q) * slot_weight[:, :, None]).astype(BF16)
    slot_rows = experts * capacity
    rows_q = lax.all_to_all(send_rows, "sp", split_axis=0, concat_axis=0, tiled=True)
    grad_q = lax.all_to_all(send_grad, "sp", split_axis=0, concat_axis=0, tiled=True)
    rows_in = join_features(rows_q.reshape(slot_rows, -1))
    grad_in = join_features(grad_q.reshape(slot_rows, -1))

    span_sums = jnp.cumsum(log_decay, axis=1)
    spot = jnp.arange(tok_rows)
    lower = (spot[:, None] >= spot[None, :])[None]
    decay = jnp.where(
        lower, jnp.exp(jnp.where(lower, span_sums[:, :, None] - span_sums[:, None, :], 0.0)), 0.0
    )
    lead = jnp.exp(span_sums)[:, :, None]
    trail = jnp.exp(span_sums[:, -1:] - span_sums)[:, :, None]
    state = state_in[:, 0].astype(BF16)
    scores = (dot("htk,hsk->hts", query_heads, key_heads) * (decay * scale)).astype(BF16)
    mixed_heads = dot("hts,hsv->htv", scores, value_heads) + lead * dot(
        "htk,hkv->htv", query_heads, state
    )
    mixed_flat = mixed_heads.astype(BF16).transpose(1, 0, 2).reshape(tok_rows, -1)
    mixed_all = lax.all_gather(mixed_flat, "sp", axis=0, tiled=True)
    totals = lax.all_gather(span_sums[:, -1], "sp", axis=0)

    gate_pre = dot("rd,df->rf", rows_in, wg)
    up_pre = dot("rd,df->rf", rows_in, wu)
    active = jax.nn.silu(gate_pre)
    hidden = (active * up_pre).astype(BF16)
    hidden_back = dot("rd,fd->rf", grad_in, wd)
    gate_back = (hidden_back * up_pre * silu_slope(gate_pre)).astype(BF16)
    up_back = (hidden_back * active).astype(BF16)
    partial_value = dot("rf,df->rd", gate_back, wg) + dot("rf,df->rd", up_back, wu)
    part = sum_features(partial_value.astype(BF16))
    down_grad = dot("rf,rd->fd", hidden, grad_in).astype(BF16)
    gate_grad = dot("rd,rf->df", rows_in, gate_back).astype(BF16)
    up_grad = dot("rd,rf->df", rows_in, up_back).astype(BF16)

    returned = lax.all_to_all(
        part.reshape(experts, capacity, -1), "sp", split_axis=0, concat_axis=0, tiled=True
    )
    mixed_q = (out_grad_q.astype(F32) + dot("ect,ecd->td", table, returned)).astype(BF16)
    mixed_grad = lax.all_gather(mixed_q, "tp", axis=1, tiled=True)

    head_grad = jnp.dot(mixed_grad, w_out, preferred_element_type=F32).astype(BF16)
    head_grad = head_grad.reshape(tok_rows, head_count, value_size).transpose(1, 0, 2)
    lead_query = (query_heads.astype(F32) * lead).astype(BF16)
    carried = dot("htk,htv->hkv", lead_query, head_grad).astype(BF16)
    carried_all = lax.all_gather(carried.reshape(1, -1, value_size), "sp", axis=0, tiled=True)
    carried_all = carried_all.reshape(spans, head_count, key_size, value_size)
    later = jnp.arange(spans)
    between = (later[None, :] < later[:, None]) & (later[None, :] > place)
    between_sum = jnp.sum(jnp.where(between[:, :, None], totals[None], 0.0), axis=1)
    weight = jnp.where((later > place)[:, None], jnp.exp(between_sum), 0.0)
    incoming = jnp.sum(carried_all.astype(F32) * weight[:, :, None, None], axis=0).astype(BF16)

    mixed_cols = lax.all_to_all(
        mixed_grad.reshape(tok_rows, spans, -1).transpose(1, 0, 2),
        "sp",
        split_axis=0,
        concat_axis=0,
        tiled=True,
    ).reshape(spans * tok_rows, -1)
    out_proj_grad = dot("td,tc->dc", mixed_cols, mixed_all)

    back_scores = (dot("htv,hsv->hts", head_grad, value_heads) * (decay * scale)).astype(BF16)
    query_gradient = dot("hts,hsk->htk", back_scores, key_heads) + lead * dot(
        "htv,hkv->htk", head_grad, state
    )
    key_grad = dot("hts,htk->hsk", back_scores, query_heads) + (trail * scale) * dot(
        "hsv,hkv->hsk", value_heads, incoming
    )
    value_grad = dot("hts,htv->hsv", scores, head_grad) + (trail * scale) * dot(
        "hsk,hkv->hsv", key_heads, incoming
    )
    return (
        gate_grad[None],
        up_grad[None],
        down_grad[None],
        out_proj_grad,
        query_gradient.astype(BF16),
        key_grad.astype(BF16),
        value_grad.astype(BF16),
    )


def solution(mesh):
    return jax.shard_map(
        body,
        mesh=mesh,
        in_specs=(
            P("sp", None),
            P("sp", None),
            P("sp", None),
            P("sp", None),
            P("sp", None, "tp"),
            P("sp", None, "tp"),
            P("sp", "tp", None),
            P(None, "tp"),
            P("tp", "sp", None),
            P("tp", "sp", None),
            P("tp", "sp", None),
            P("tp", "sp"),
            P("tp", "sp", None, None),
        ),
        out_specs=(
            P("sp", None, "tp"),
            P("sp", None, "tp"),
            P("sp", "tp", None),
            P("sp", "tp"),
            P("tp", "sp", None),
            P("tp", "sp", None),
            P("tp", "sp", None),
        ),
        check_vma=False,
    )
```

time: 336 us -> 196 us (0.58)
  waiting for transfers between devices: 113 us -> 43.3 us
  local copies, waits for them, and re-layouts: 45.8 us -> 7.87 us
  blocking collectives: 56.3 us -> 82.5 us
  matrix products: 58.2 us -> 33.3 us
  other arithmetic: 33.1 us -> 8.48 us
  starting transfers between devices: 11.9 us -> 4.31 us
    reduce_scatter x1 -> x0, waiting for transfers between devices: 54.1 us -> none  [body(): lax.psum_scatter(lax.dot_general(mixed_grad, mixed_flat, (((0,), (0,)), (...]
    all_to_all x2 -> x1, waiting for transfers between devices: 48.3 us -> 18.2 us  [body(): lax.all_to_all(mixed_grad.reshape(tok_rows, spans, -1).transpose(1, 0, 2)...]
    dot_general x39 -> x25, matrix products: 58.2 us -> 33.3 us  [the longest x24 32.6 us: dot(): return jnp.einsum(spec, a, b, preferred_element_type=F32)]
    all_to_all x2 -> x3, blocking collectives: 34.5 us -> 56.1 us  [the longest x1 24.2 us: body(): lax.all_to_all(part.reshape(experts, capacity, -1), 'sp', split_axis=0, c...]
    gather x4 -> x0, local copies, waits for them, and re-layouts: 13.3 us -> none  [the longest x1 4.82 us: body(): returned.reshape(experts * capacity, model_width)[target]]
    ppermute x0 -> x2, waiting for transfers between devices: none -> 11.7 us  [exchange(): return lax.ppermute(array, axis, [(i, i ^ step) for i in range(count)])]
    all_to_all x2 -> x1, starting transfers between devices: 11.6 us -> 3.5 us  [body(): lax.all_to_all(mixed_grad.reshape(tok_rows, spans, -1).transpose(1, 0, 2)...]
    add x7 -> x0, other arithmetic: 7.94 us -> none  [link_states(): lower_part[1] + lower_part[0][:, None, None] * higher_part[1]]
  transfers between devices with their start and end apart: 5 -> 7, of which waited for: 4 -> 4; matrix products, arithmetic and copies ran while one was open for 24% -> 21% of each run, Pallas kernels for 0% -> 0%
where the time goes in v1:
time: 196 us; the launch traced here: 195 us
  blocking collectives  82.5 us (42%)
  waiting for transfers between devices  43.3 us (22%)
  matrix products  33.3 us (17%)
  between operations  15.1 us (8%)
  other arithmetic  8.48 us (4%)
  local copies, waits for them, and re-layouts  7.87 us (4%)
  starting transfers between devices  4.31 us (2%)
    dot_general x24, matrix products, dot(): return jnp.einsum(spec, a, b, preferred_element_type=F32)  32.6 us
    all_to_all x1, blocking collectives, body(): lax.all_to_all(part.reshape(experts, capacity, -1), 'sp', split_axis=0, c...  24.2 us
    unnamed x1, blocking collectives  19.8 us
    all_to_all x1, blocking collectives, body(): lax.all_to_all(send_rows, 'sp', split_axis=0, concat_axis=0, tiled=True)  18.2 us
    all_to_all x1, waiting for transfers between devices, body(): lax.all_to_all(mixed_grad.reshape(tok_rows, spans, -1).transpose(1, 0, 2)...  18.2 us
    all_to_all x1, blocking collectives, body(): lax.all_to_all(send_grad, 'sp', split_axis=0, concat_axis=0, tiled=True)  13.7 us
    all_gather x2, waiting for transfers between devices, join_features(): gathered = lax.all_gather(rows, 'tp', axis=0)  13.3 us
    ppermute x2, waiting for transfers between devices, exchange(): return lax.ppermute(array, axis, [(i, i ^ step) for i in range(count)])  11.7 us
  transfers between devices with their start and end apart: 7, of which 4 were waited for; matrix products, arithmetic and copies ran while one was open for 21% of the time, Pallas kernels for 0%

profile of v1, /device:TPU:0, one launch (start us, length us, event | category | flops | bytes accessed | tf_op | source)
XLA Modules:
  0.0 194.8 jit_solution(5836768791151627611)
XLA Ops:
  7.3 0.8 fusion.57
  8.3 1.2 convolution_convert_fusion.3
  9.4 18.2 %all_to_all.20 = bf16[8,40,512]{2,1,0:T(8,128)(2,1)} all-to-all(bf16[8,40,512]{2,1,0:T(8,128)(2,1)S(1)} %convolution_convert_fusion.3), channel_id=1, replica_groups=mesh['sp'=8,'tp'=4] {'sp'}, dimensions={0} | all-to-all | bytes 655360 | tf_op jit(solution)/shard_map/all_to_all | solution.py:95
  27.7 0.7 select_reduce_fusion.2
  28.6 1.1 fusion.17
  29.7 13.7 %all_to_all.21 = bf16[8,40,512]{2,1,0:T(8,128)(2,1)} all-to-all(bf16[8,40,512]{2,1,0:T(8,128)(2,1)S(1)} %fusion.17), channel_id=1, replica_groups=mesh['sp'=8,'tp'=4] {'sp'}, dimensions={0} | all-to-all | bytes 655360 | tf_op jit(solution)/shard_map/all_to_all | solution.py:96
  43.5 0.3 reduce_window_sum.11
  44.1 0.7 exponential_multiply_fusion
  45.4 0.8 copy.52
  46.4 1.5 slice_bitcast_fusion.9
  48.0 0.4 copy-done.2
  48.4 0.8 fusion.9
  49.3 1.7 fusion.6
  51.0 13.2 %all-gather.8.cloned.1.call-done = bf16[4,320,512]{2,1,0:T(8,128)(2,1)} async-done(((bf16[1,320,512]{2,1,0:T(8,128)(2,1)}), bf16[4,320,512]{2,1,0:T(8,128)(2,1)}) %all-gather.8.cloned.1.call-update) | async-done | bytes 1310736 | tf_op jit(solution)/shard_map/all_gather | solution.py:34
  64.2 1.5 slice_bitcast_fusion.5
  65.8 0.4 copy-done.36
  66.2 2.1 %multiply_convert_fusion.1 = (bf16[320,512]{1,0:T(8,128)(2,1)S(1)}, bf16[320,512]{1,0:T(8,128)(2,1)S(1)}) fusion(f32[320,512]{1,0:T(8,128)} %fusion.6, f32[320,512]{1,0:T(8,128)S(1)} %fusion.9, bf16[1,512,2048]{2,1,0:T(8,128)(2,1)S(1)} %copy-done.36, bf16[320,512]{1,0:T(8,128)(2,1)S(1)} %get-tuple-element.12, bf16[320,512]{1,0:T(8,128)(2,1)S(1)} %get-tuple-element.13, ...), kind=kOutput, calls=%fused_computation.56 | convolution fusion | flops 678461440 | bytes 5373952 | tf_op jit(solution)/shard_map/rd,fd->rf/dot_general | solution.py:11
  68.4 0.9 fusion.4
  69.3 0.9 copy-done.3
  70.2 0.9 fusion.3
  71.2 0.9 pad_maximum_fusion.2
  72.3 2.2 %collective-permute-done = bf16[2,320,512]{2,1,0:T(8,128)(2,1)} collective-permute-done((bf16[2,320,512]{2,1,0:T(8,128)(2,1)}, bf16[2,320,512]{2,1,0:T(8,128)(2,1)}, u32[]{:S(2)}, u32[]{:S(2)}) %collective-permute-start) | collective-permute-done | bytes 655392 | tf_op jit(solution)/shard_map/ppermute | solution.py:40
  74.5 1.3 fusion.31
  75.9 0.4 collective-permute-start.1
  76.3 9.5 %collective-permute-done.1 = bf16[1,320,512]{2,1,0:T(8,128)(2,1)S(1)} collective-permute-done((bf16[1,320,512]{2,1,0:T(8,128)(2,1)S(1)}, bf16[1,320,512]{2,1,0:T(8,128)(2,1)S(1)}, u32[]{:S(2)}, u32[]{:S(2)}) %collective-permute-start.1) | collective-permute-done | bytes 327712 | tf_op jit(solution)/shard_map/ppermute | solution.py:40
  85.8 1.4 fusion.29
  87.1 24.2 %all_to_all.22 = bf16[8,40,512]{2,1,0:T(8,128)(2,1)S(1)} all-to-all(bf16[8,40,512]{2,1,0:T(8,128)(2,1)S(1)} %bitcast.167), channel_id=1, replica_groups=mesh['sp'=8,'tp'=4] {'sp'}, dimensions={0} | all-to-all | bytes 655360 | tf_op jit(solution)/shard_map/all_to_all | solution.py:130
  111.3 1.2 fusion.24
  112.5 6.5 %all_gather.20 = bf16[128,2048]{1,0:T(8,128)(2,1)S(1)} all-gather(bf16[128,512]{1,0:T(8,128)(2,1)S(1)} %fusion.24), channel_id=1, replica_groups=mesh['sp'=8,'tp'=4] {'tp'}, dimensions={1}, use_global_device_ids=true | all-gather | bytes 655360 | tf_op jit(solution)/shard_map/all_gather | solution.py:134
  119.0 0.7 convolution_convert_fusion.5
  119.8 1.1 convolution_convert_fusion.4
  120.9 0.6 dynamic-slice
  122.4 19.8 %all-reduce = f32[32]{0:T(128)S(1)} all-reduce(f32[32]{0:T(128)S(1)} %dynamic-update-slice), channel_id=2, replica_groups=mesh['sp'=8,'tp'=4] {'sp'}, use_global_device_ids=true, to_apply=%add | all-reduce | flops 32 | bytes 256
  142.6 4.1 %fusion.1 = bf16[1,2048,512]{2,1,0:T(8,128)(2,1)} fusion(bf16[320,512]{1,0:T(8,128)(2,1)} %copy-done.14, bf16[320,512]{1,0:T(8,128)(2,1)} %copy-done.17, bf16[320,512]{1,0:T(8,128)(2,1)} %copy-done.19, bf16[320,512]{1,0:T(8,128)(2,1)} %copy-done.21, bf16[320,512]{1,0:T(8,128)(2,1)} %copy-done.15), kind=kOutput, calls=%fused_computation.6 | convolution fusion | flops 677380096 | bytes 3735552 | tf_op jit(solution)/shard_map/rd,rf->df/dot_general | solution.py:11
  146.8 2.6 %fusion = bf16[1,2048,512]{2,1,0:T(8,128)(2,1)} fusion(bf16[320,512]{1,0:T(8,128)(2,1)S(1)} %copy-done.10, bf16[320,512]{1,0:T(8,128)(2,1)S(1)} %copy-done.18, bf16[320,512]{1,0:T(8,128)(2,1)S(1)} %copy-done.20, bf16[320,512]{1,0:T(8,128)(2,1)S(1)} %copy-done.22, bf16[320,512]{1,0:T(8,128)(2,1)S(1)} %copy-done.16), kind=kOutput, calls=%fused_computation.5 | convolution fusion | flops 677380096 | bytes 3735552 | tf_op jit(solution)/shard_map/rd,rf->df/dot_general | solution.py:11
  149.4 2.6 %fusion.2 = bf16[1,512,2048]{2,1,0:T(8,128)(2,1)} fusion(f32[320,512]{1,0:T(8,128)S(1)} %copy-done.39, bf16[320,512]{1,0:T(8,128)(2,1)S(1)} %copy-done.26, bf16[320,512]{1,0:T(8,128)(2,1)S(1)} %copy-done.28, bf16[320,512]{1,0:T(8,128)(2,1)S(1)} %copy-done.30, bf16[320,512]{1,0:T(8,128)(2,1)S(1)} %copy-done.24, f32[320,512]{1,0:T(8,128)S(1)} %copy-done.40), kind=kOutput, calls=%fused_computation.7 | convolution fusion | flops 678363136 | bytes 4718592 | tf_op jit(solution)/shard_map/rf,rd->fd/dot_general | solution.py:11
  152.1 0.8 copy.86
  152.9 3.5 %all-to-all-start.3 = ((bf16[8,128,256]{2,1,0:T(8,128)(2,1)}), bf16[8,128,256]{2,1,0:T(8,128)(2,1)S(1)}, u32[]{:S(2)}, u32[]{:S(2)}) async-start(bf16[8,128,256]{2,1,0:T(8,128)(2,1)} %bitcast.166), calls=%async_computation.3 | async-start | bytes 1048576 | tf_op jit(solution)/shard_map/all_to_all | solution.py:148
  156.4 1.2 fusion.26
  157.6 1.0 fusion.66
  158.6 1.1 fusion.65
  159.6 1.2 fusion.32
  160.8 1.9 fusion.27
  162.8 18.2 %all-to-all-done.3 = bf16[8,128,256]{2,1,0:T(8,128)(2,1)S(1)} async-done(((bf16[8,128,256]{2,1,0:T(8,128)(2,1)}), bf16[8,128,256]{2,1,0:T(8,128)(2,1)S(1)}, u32[]{:S(2)}, u32[]{:S(2)}) %all-to-all-start.3) | async-done | bytes 524320 | tf_op jit(solution)/shard_map/all_to_all | solution.py:148
  181.0 3.3 %fusion.64 = f32[256,1024]{1,0:T(8,128)} fusion(bf16[1024,256]{1,0:T(8,128)(2,1)S(1)} %bitcast.165, bf16[1024,1024]{0,1:T(8,128)(2,1)} %all-gather.10.cloned.1.call-done), kind=kOutput, calls=%fused_computation.121 | convolution fusion | flops 536870912 | bytes 3670016 | tf_op jit(solution)/shard_map/td,tc->dc/dot_general | solution.py:11
  184.3 2.1 %multiply_reduce_fusion = bf16[512,256]{1,0:T(8,128)(2,1)S(1)} fusion(bf16[8,512,256]{2,1,0:T(8,128)(2,1)} %all-gather.12.cloned.1.call-done, f32[8,512]{1,0:T(8,128)S(1)} %broadcast_bitcast_fusion), kind=kLoop, calls=%fused_computation | loop fusion | flops 3014656 | bytes 2375680 | tf_op jit(solution)/shard_map/reduce_sum | solution.py:146
  186.4 0.9 fusion.18
  187.4 0.9 fusion.28
  (108 shorter events, 2.5 us)
Async XLA Ops:
  7.2 42.1 %copy-start = (bf16[1,2048,512]{2,1,0:T(8,128)(2,1)S(1)}, bf16[1,2048,512]{2,1,0:T(8,128)(2,1)}, u32[]{:S(2)}) copy-start(bf16[1,2048,512]{2,1,0:T(8,128)(2,1)} %param.17) | copy-start | bytes 6291460
  7.2 36.3 %copy-start.35 = (f32[4,128]{1,0:T(4,128)S(1)}, f32[4,128]{1,0:T(4,128)}, u32[]{:S(2)}) copy-start(f32[4,128]{1,0:T(4,128)} %param.24) | copy-start | bytes 6148
  7.2 37.5 %copy-start.5 = (bf16[4,128,128]{2,1,0:T(8,128)(2,1)S(1)}, bf16[4,128,128]{2,1,0:T(8,128)(2,1)}, u32[]{:S(2)}) copy-start(bf16[4,128,128]{2,1,0:T(8,128)(2,1)} %param.21) | copy-start | bytes 393220
  7.2 37.5 %copy-start.12 = (bf16[4,128,128]{2,1,0:T(8,128)(2,1)S(1)}, bf16[4,128,128]{2,1,0:T(8,128)(2,1)}, u32[]{:S(2)}) copy-start(bf16[4,128,128]{2,1,0:T(8,128)(2,1)} %param.22) | copy-start | bytes 393220
  7.2 37.7 %copy-start.4 = (f32[4,1,128,256]{3,2,1,0:T(8,128)S(1)}, f32[4,1,128,256]{3,2,1,0:T(8,128)}, u32[]{:S(2)}) copy-start(f32[4,1,128,256]{3,2,1,0:T(8,128)} %param.25) | copy-start | bytes 1572868
  7.2 39.2 %all-gather.6.cloned.1.call-start = ((), (), s32[]{:S(2)}) async-start(), calls=%async_computation.4 | async-start | bytes 1638400 | tf_op jit(solution)/shard_map/all_gather | solution.py:34
  9.4 35.8 %copy-start.7 = (bf16[4,128,256]{2,1,0:T(8,128)(2,1)S(1)}, bf16[4,128,256]{2,1,0:T(8,128)(2,1)}, u32[]{:S(2)}) copy-start(bf16[4,128,256]{2,1,0:T(8,128)(2,1)} %param.23) | copy-start | bytes 786436
  27.7 36.5 %all-gather.8.cloned.1.call-start = ((), (), s32[]{:S(2)}) async-start(), calls=%async_computation.5 | async-start | bytes 1638400 | tf_op jit(solution)/shard_map/all_gather | solution.py:34
  43.5 119.3 %all-gather.10.cloned.1.call-start = ((), (), s32[]{:S(2)}) async-start(), calls=%async_computation.6 | async-start | bytes 2359296 | tf_op jit(solution)/shard_map/all_gather | solution.py:114
  43.8 2.5 %copy-start.33 = (f32[4,128]{1,0:T(4,128)}, f32[4,128]{1,0:T(4,128)S(1)}, u32[]{:S(2)}) copy-start(f32[4,128]{1,0:T(4,128)S(1)} %reduce_window_sum.11) | copy-start | bytes 6148
  44.0 2.3 %copy-start.34 = (pred[128,128]{1,0:T(8,128)(4,1)}, pred[128,128]{1,0:T(8,128)(4,1)S(1)}, u32[]{:S(2)}) copy-start(pred[128,128]{1,0:T(8,128)(4,1)S(1)} %iota_compare_fusion.1) | copy-start | bytes 49156
  44.7 75.0 %copy-start.32 = (f32[4,128]{1,0:T(4,128)}, f32[4,128]{1,0:T(4,128)S(1)}, u32[]{:S(2)}) copy-start(f32[4,128]{1,0:T(4,128)S(1)} %get-tuple-element.21) | copy-start | bytes 6148
  44.9 3.0 %copy-start.11 = (bf16[4,128,128]{2,1,0:T(8,128)(2,1)}, bf16[4,128,128]{2,1,0:T(8,128)(2,1)S(1)}, u32[]{:S(2)}) copy-start(bf16[4,128,128]{2,1,0:T(8,128)(2,1)S(1)} %fusion.25) | copy-start | bytes 393220
  46.3 138.0 %all-gather.12.cloned.1.call-start = ((), (), s32[]{:S(2)}) async-start(), calls=%async_computation.7 | async-start | bytes 2359296 | tf_op jit(solution)/shard_map/all_gather | solution.py:140
  46.4 2.0 %copy-start.2 = (bf16[1,2048,512]{2,1,0:T(8,128)(2,1)S(1)}, bf16[1,2048,512]{2,1,0:T(8,128)(2,1)}, u32[]{:S(2)}) copy-start(bf16[1,2048,512]{2,1,0:T(8,128)(2,1)} %param.18) | copy-start | bytes 6291460
  47.9 1.3 copy-start.15
  47.9 1.3 copy-start.17
  47.9 1.3 copy-start.19
  48.0 1.3 copy-start.21
  49.3 16.5 %copy-start.38 = (f32[320,512]{1,0:T(8,128)}, f32[320,512]{1,0:T(8,128)S(1)}, u32[]{:S(2)}) copy-start(f32[320,512]{1,0:T(8,128)S(1)} %fusion.9) | copy-start | bytes 1966084
  64.2 2.0 %copy-start.36 = (bf16[1,512,2048]{2,1,0:T(8,128)(2,1)S(1)}, bf16[1,512,2048]{2,1,0:T(8,128)(2,1)}, u32[]{:S(2)}) copy-start(bf16[1,512,2048]{2,1,0:T(8,128)(2,1)} %param.19) | copy-start | bytes 6291460
  65.7 2.6 %copy-start.23 = (bf16[320,512]{1,0:T(8,128)(2,1)}, bf16[320,512]{1,0:T(8,128)(2,1)S(1)}, u32[]{:S(2)}) copy-start(bf16[320,512]{1,0:T(8,128)(2,1)S(1)} %get-tuple-element.11) | copy-start | bytes 983044
  65.7 2.6 %copy-start.25 = (bf16[320,512]{1,0:T(8,128)(2,1)}, bf16[320,512]{1,0:T(8,128)(2,1)S(1)}, u32[]{:S(2)}) copy-start(bf16[320,512]{1,0:T(8,128)(2,1)S(1)} %get-tuple-element.12) | copy-start | bytes 983044
  65.7 2.6 %copy-start.27 = (bf16[320,512]{1,0:T(8,128)(2,1)}, bf16[320,512]{1,0:T(8,128)(2,1)S(1)}, u32[]{:S(2)}) copy-start(bf16[320,512]{1,0:T(8,128)(2,1)S(1)} %get-tuple-element.13) | copy-start | bytes 983044
  65.7 2.6 %copy-start.29 = (bf16[320,512]{1,0:T(8,128)(2,1)}, bf16[320,512]{1,0:T(8,128)(2,1)S(1)}, u32[]{:S(2)}) copy-start(bf16[320,512]{1,0:T(8,128)(2,1)S(1)} %get-tuple-element.14) | copy-start | bytes 983044
  68.4 0.9 copy-start.9
  68.4 0.9 copy-start.14
  68.4 1.8 copy-start.3
  72.1 2.4 %collective-permute-start = (bf16[2,320,512]{2,1,0:T(8,128)(2,1)}, bf16[2,320,512]{2,1,0:T(8,128)(2,1)}, u32[]{:S(2)}, u32[]{:S(2)}) collective-permute-start(bf16[2,320,512]{2,1,0:T(8,128)(2,1)} %pad_maximum_fusion.2), channel_id=1, source_target_pairs={{0,1},{1,0},{2,3},{3,2},{4,5},{5,4},{6,7},{7,6},{8,9},{9,8},{10,11... | collective-permute-start | bytes 1966088 | tf_op jit(solution)/shard_map/ppermute | solution.py:40
  75.8 43.2 %copy-start.1 = (bf16[2048,1024]{1,0:T(8,128)(2,1)S(1)}, bf16[2048,1024]{1,0:T(8,128)(2,1)}, u32[]{:S(2)}) copy-start(bf16[2048,1024]{1,0:T(8,128)(2,1)} %param.20) | copy-start | bytes 12582916
  75.9 9.9 %collective-permute-start.1 = (bf16[1,320,512]{2,1,0:T(8,128)(2,1)S(1)}, bf16[1,320,512]{2,1,0:T(8,128)(2,1)S(1)}, u32[]{:S(2)}, u32[]{:S(2)}) collective-permute-start(bf16[1,320,512]{2,1,0:T(8,128)(2,1)S(1)} %fusion.31), channel_id=1, source_target_pairs={{0,2},{1,3},{2,0},{3,1},{4,6},{5,7},{6,4},{7,5},{8,10},{9,11},{10,... | collective-permute-start | bytes 983048 | tf_op jit(solution)/shard_map/ppermute | solution.py:40
  119.0 1.9 copy-start.37
  142.6 4.1 %copy-start.10 = (bf16[320,512]{1,0:T(8,128)(2,1)S(1)}, bf16[320,512]{1,0:T(8,128)(2,1)}, u32[]{:S(2)}) copy-start(bf16[320,512]{1,0:T(8,128)(2,1)} %copy-done.9) | copy-start | bytes 983044
  142.6 4.1 %copy-start.16 = (bf16[320,512]{1,0:T(8,128)(2,1)S(1)}, bf16[320,512]{1,0:T(8,128)(2,1)}, u32[]{:S(2)}) copy-start(bf16[320,512]{1,0:T(8,128)(2,1)} %copy-done.15) | copy-start | bytes 983044
  142.6 4.1 %copy-start.18 = (bf16[320,512]{1,0:T(8,128)(2,1)S(1)}, bf16[320,512]{1,0:T(8,128)(2,1)}, u32[]{:S(2)}) copy-start(bf16[320,512]{1,0:T(8,128)(2,1)} %copy-done.17) | copy-start | bytes 983044
  142.6 4.1 %copy-start.20 = (bf16[320,512]{1,0:T(8,128)(2,1)S(1)}, bf16[320,512]{1,0:T(8,128)(2,1)}, u32[]{:S(2)}) copy-start(bf16[320,512]{1,0:T(8,128)(2,1)} %copy-done.19) | copy-start | bytes 983044
  142.6 4.1 %copy-start.22 = (bf16[320,512]{1,0:T(8,128)(2,1)S(1)}, bf16[320,512]{1,0:T(8,128)(2,1)}, u32[]{:S(2)}) copy-start(bf16[320,512]{1,0:T(8,128)(2,1)} %copy-done.21) | copy-start | bytes 983044
  146.7 2.7 %copy-start.24 = (bf16[320,512]{1,0:T(8,128)(2,1)S(1)}, bf16[320,512]{1,0:T(8,128)(2,1)}, u32[]{:S(2)}) copy-start(bf16[320,512]{1,0:T(8,128)(2,1)} %copy-done.23) | copy-start | bytes 983044
  146.7 2.7 %copy-start.26 = (bf16[320,512]{1,0:T(8,128)(2,1)S(1)}, bf16[320,512]{1,0:T(8,128)(2,1)}, u32[]{:S(2)}) copy-start(bf16[320,512]{1,0:T(8,128)(2,1)} %copy-done.25) | copy-start | bytes 983044
  146.7 2.7 %copy-start.28 = (bf16[320,512]{1,0:T(8,128)(2,1)S(1)}, bf16[320,512]{1,0:T(8,128)(2,1)}, u32[]{:S(2)}) copy-start(bf16[320,512]{1,0:T(8,128)(2,1)} %copy-done.27) | copy-start | bytes 983044
  146.7 2.6 %copy-start.30 = (bf16[320,512]{1,0:T(8,128)(2,1)S(1)}, bf16[320,512]{1,0:T(8,128)(2,1)}, u32[]{:S(2)}) copy-start(bf16[320,512]{1,0:T(8,128)(2,1)} %copy-done.29) | copy-start | bytes 983044
  146.8 2.6 %copy-start.39 = (f32[320,512]{1,0:T(8,128)S(1)}, f32[320,512]{1,0:T(8,128)}, u32[]{:S(2)}) copy-start(f32[320,512]{1,0:T(8,128)} %copy-done.38) | copy-start | bytes 1966084
  146.8 2.6 %copy-start.40 = (f32[320,512]{1,0:T(8,128)S(1)}, f32[320,512]{1,0:T(8,128)}, u32[]{:S(2)}) copy-start(f32[320,512]{1,0:T(8,128)} %fusion.6) | copy-start | bytes 1966084
  152.9 28.1 %all-to-all-start.3 = ((bf16[8,128,256]{2,1,0:T(8,128)(2,1)}), bf16[8,128,256]{2,1,0:T(8,128)(2,1)S(1)}, u32[]{:S(2)}, u32[]{:S(2)}) async-start(bf16[8,128,256]{2,1,0:T(8,128)(2,1)} %bitcast.166), calls=%async_computation.3 | async-start | bytes 1048576 | tf_op jit(solution)/shard_map/all_to_all | solution.py:148
  184.3 2.1 %copy-start.13 = (bf16[4,128,128]{2,1,0:T(8,128)(2,1)S(1)}, bf16[4,128,128]{2,1,0:T(8,128)(2,1)}, u32[]{:S(2)}) copy-start(bf16[4,128,128]{2,1,0:T(8,128)(2,1)} %param.22) | copy-start | bytes 393220
  184.3 2.1 %copy-start.31 = (f32[4,128]{1,0:T(4,128)S(1)}, f32[4,128]{1,0:T(4,128)}, u32[]{:S(2)}) copy-start(f32[4,128]{1,0:T(4,128)} %get-tuple-element.19) | copy-start | bytes 6148
  184.3 3.1 %copy-start.6 = (f32[4,128,128]{2,1,0:T(8,128)S(1)}, f32[4,128,128]{2,1,0:T(8,128)}, u32[]{:S(2)}) copy-start(f32[4,128,128]{2,1,0:T(8,128)} %fusion.66) | copy-start | bytes 786436
  184.3 3.1 %copy-start.8 = (bf16[4,128,256]{2,1,0:T(8,128)(2,1)S(1)}, bf16[4,128,256]{2,1,0:T(8,128)(2,1)}, u32[]{:S(2)}) copy-start(bf16[4,128,256]{2,1,0:T(8,128)(2,1)} %param.23) | copy-start | bytes 786436
Sparse Core Ops, SparseCore 0:
  27.8 16.6 all-gather.5
  46.0 18.1 all-gather.7
  66.8 54.6 all-gather.9
  123.5 57.8 all-gather.11

commit v2 on v1

--- a/solution.py
+++ b/solution.py
@@ -1,6 +1,8 @@
 import jax
 import jax.numpy as jnp
 from jax import lax
+from jax.experimental import pallas as pl
+from jax.experimental.pallas import tpu as pltpu
 from jax.sharding import PartitionSpec as P
 
 F32 = jnp.float32
@@ -30,30 +32,220 @@
     return lax.dynamic_slice_in_dim(array, lax.axis_index(axis_name) * width, width, axis)
 
 
-def join_features(rows):
-    gathered = lax.all_gather(rows, "tp", axis=0)
-    return jnp.concatenate([gathered[i] for i in range(gathered.shape[0])], axis=1)
-
-
-def exchange(array, axis, step):
-    count = lax.axis_size(axis)
-    return lax.ppermute(array, axis, [(i, i ^ step) for i in range(count)])
-
-
-def sum_features(value):
-    count = lax.axis_size("tp")
-    place = lax.axis_index("tp")
-    width = value.shape[1] // count
-    parts = [value[:, i * width : (i + 1) * width] for i in range(count)]
-    step = 1
-    while len(parts) > 1:
-        upper = (place // step) % 2 == 1
-        keep = [jnp.where(upper, b, a) for a, b in zip(parts[::2], parts[1::2])]
-        send = [jnp.where(upper, a, b).astype(BF16) for a, b in zip(parts[::2], parts[1::2])]
-        got = exchange(jnp.stack(send), "tp", step)
-        parts = [k.astype(F32) + got[i].astype(F32) for i, k in enumerate(keep)]
-        step *= 2
-    return parts[0].astype(BF16)
+MESH = pl.DeviceIdType.MESH
+VMEM = pl.BlockSpec(memory_space=pltpu.VMEM)
+
+
+def greet(peers):
+    barrier = pltpu.get_barrier_semaphore()
+    for peer in peers:
+        pl.semaphore_signal(barrier, inc=1, device_id=peer, device_id_type=MESH)
+    pl.semaphore_wait(barrier, len(peers))
+
+
+def places():
+    spans, place = lax.axis_size("sp"), lax.axis_index("sp")
+    members, member = lax.axis_size("tp"), lax.axis_index("tp")
+    sp_peers = [None] + [
+        {"sp": lax.rem(place + k, spans), "tp": member} for k in range(1, spans)
+    ]
+    rows = [
+        {"sp": place, "tp": lax.rem(member + 2 * j, members)} for j in range(1, members // 2)
+    ]
+    partner = {"sp": place, "tp": member + 1 - 2 * lax.rem(member, 2)}
+    return spans, place, members, member, sp_peers, [None] + rows, partner
+
+
+def remote(src, dst, send, recv, peer):
+    return pltpu.make_async_remote_copy(
+        src_ref=src, dst_ref=dst, send_sem=send, recv_sem=recv, device_id=peer, device_id_type=MESH
+    )
+
+
+def dispatch_kernel(x, out, own, sp_send, sp_recv, y_send, y_recv, c_send, c_recv):
+    spans, place, members, member, sp_peers, y_peers, partner = places()
+    chips = members // 2
+    greet(sp_peers[1:] + y_peers[1:] + [partner])
+    pending = []
+    arrivals = [pltpu.make_async_copy(x.at[place], out.at[member, place], own)]
+    arrivals[0].start()
+    for k in range(1, spans):
+        copy = remote(
+            x.at[lax.rem(place + k, spans)],
+            out.at[member, place],
+            sp_send.at[k],
+            sp_recv.at[k],
+            sp_peers[k],
+        )
+        copy.start()
+        arrivals.append(copy)
+
+    def pass_on(j, k):
+        source = lax.rem(place + spans - k, spans)
+        owner = lax.rem(member + members - 2 * j, members)
+        block = out.at[owner, source]
+        copy = remote(block, block, c_send.at[j, k], c_recv.at[j, k], partner)
+        copy.start()
+        pending.append(copy)
+
+    flights = {}
+    for k in range(spans + 1):
+        if k < spans:
+            if k == 0:
+                arrivals[0].wait()
+            else:
+                arrivals[k].wait_recv()
+            source = lax.rem(place + spans - k, spans)
+            block = out.at[member, source]
+            for j in range(1, chips):
+                copy = remote(block, block, y_send.at[j, k], y_recv.at[j, k], y_peers[j])
+                copy.start()
+                flights[j, k] = copy
+            pass_on(0, k)
+        if k > 0:
+            for j in range(1, chips):
+                flights[j, k - 1].wait_recv()
+                pass_on(j, k - 1)
+    for copy in pending:
+        copy.wait_recv()
+    for copy in arrivals[1:] + list(flights.values()) + pending:
+        copy.wait_send()
+
+
+def dispatch(rows):
+    spans, members = lax.axis_size("sp"), lax.axis_size("tp")
+    dma = pltpu.SemaphoreType.DMA
+    return pl.pallas_call(
+        dispatch_kernel,
+        out_shape=jax.ShapeDtypeStruct((members,) + rows.shape, rows.dtype),
+        in_specs=[VMEM],
+        out_specs=VMEM,
+        scratch_shapes=[dma, dma((spans,)), dma((spans,))]
+        + [dma((members // 2, spans)) for _ in range(4)],
+        cost_estimate=pl.CostEstimate(flops=0, bytes_accessed=60 << 20, transcendentals=0),
+        compiler_params=pltpu.CompilerParams(collective_id=0, has_side_effects=True),
+    )(rows)
+
+
+def swap_kernel(x, out, own, sp_send, sp_recv):
+    spans, place, _, _, sp_peers, _, _ = places()
+    greet(sp_peers[1:])
+    mine = pltpu.make_async_copy(x.at[place], out.at[place], own)
+    mine.start()
+    copies = []
+    for k in range(1, spans):
+        copy = remote(
+            x.at[lax.rem(place + k, spans)], out.at[place], sp_send.at[k], sp_recv.at[k], sp_peers[k]
+        )
+        copy.start()
+        copies.append(copy)
+    mine.wait()
+    for copy in copies:
+        copy.wait()
+
+
+def swap(blocks):
+    spans = lax.axis_size("sp")
+    dma = pltpu.SemaphoreType.DMA
+    return pl.pallas_call(
+        swap_kernel,
+        out_shape=jax.ShapeDtypeStruct(blocks.shape, blocks.dtype),
+        in_specs=[VMEM],
+        out_specs=VMEM,
+        scratch_shapes=[dma, dma((spans,)), dma((spans,))],
+        cost_estimate=pl.CostEstimate(flops=0, bytes_accessed=30 << 20, transcendentals=0),
+        compiler_params=pltpu.CompilerParams(collective_id=1, has_side_effects=True),
+    )(blocks)
+
+
+def combine_kernel(
+    x, out, from_core, pair, from_y, total, own, c_send, c_recv, y_send, y_recv, sp_send, sp_recv
+):
+    spans, place, members, member, sp_peers, y_peers, partner = places()
+    chips = members // 2
+    core = lax.rem(member, 2)
+    chip = member // 2
+    greet(sp_peers[1:] + y_peers[1:] + [partner])
+    order = [lax.rem(place + k + 1, spans) for k in range(spans)]
+    core_copies = {}
+    for k in range(spans):
+        for m in range(chips):
+            copy = remote(
+                x.at[2 * m + 1 - core, order[k]],
+                from_core.at[m, order[k]],
+                c_send.at[m, k],
+                c_recv.at[m, k],
+                partner,
+            )
+            copy.start()
+            core_copies[m, k] = copy
+    y_copies = {}
+    sp_copies = []
+
+    def send_y(k):
+        for j in range(1, chips):
+            copy = remote(
+                pair.at[lax.rem(chip + j, chips), order[k]],
+                from_y.at[j, order[k]],
+                y_send.at[j, k],
+                y_recv.at[j, k],
+                y_peers[j],
+            )
+            copy.start()
+            y_copies[j, k] = copy
+
+    def send_sp(k):
+        if k == spans - 1:
+            return
+        copy = remote(
+            total.at[order[k]], out.at[place], sp_send.at[k], sp_recv.at[k], sp_peers[k + 1]
+        )
+        copy.start()
+        sp_copies.append(copy)
+
+    for k in range(spans + 1):
+        if k < spans:
+            for m in range(chips):
+                core_copies[m, k].wait_recv()
+                pair[m, order[k]] = (
+                    x[2 * m + core, order[k]].astype(F32) + from_core[m, order[k]].astype(F32)
+                ).astype(BF16)
+        if k > 0:
+            send_y(k - 1)
+    for k in range(spans + 1):
+        if k < spans:
+            value = pair[chip, order[k]].astype(F32)
+            for j in range(1, chips):
+                y_copies[j, k].wait_recv()
+                value = value + from_y[j, order[k]].astype(F32)
+            total[order[k]] = value.astype(BF16)
+        if k > 0:
+            send_sp(k - 1)
+    mine = pltpu.make_async_copy(total.at[place], out.at[place], own)
+    mine.start()
+    mine.wait()
+    for copy in sp_copies:
+        copy.wait_recv()
+    for copy in sp_copies + list(y_copies.values()) + list(core_copies.values()):
+        copy.wait_send()
+
+
+def combine(parts):
+    members, spans, rows, width = parts.shape
+    dma = pltpu.SemaphoreType.DMA
+    chips = members // 2
+    slots = pltpu.VMEM((chips, spans, rows, width), BF16)
+    return pl.pallas_call(
+        combine_kernel,
+        out_shape=jax.ShapeDtypeStruct((spans, rows, width), BF16),
+        in_specs=[VMEM],
+        out_specs=VMEM,
+        scratch_shapes=[slots, slots, slots, pltpu.VMEM((spans, rows, width), BF16), dma]
+        + [dma((chips, spans)) for _ in range(4)]
+        + [dma((spans,)) for _ in range(2)],
+        cost_estimate=pl.CostEstimate(flops=0, bytes_accessed=45 << 20, transcendentals=0),
+        compiler_params=pltpu.CompilerParams(collective_id=2, has_side_effects=True),
+    )(parts)
 
 
 def silu_slope(gate_pre):
@@ -92,11 +284,6 @@
     send_rows = dot("ect,td->ecd", table, quarter(moe_input, "tp", 1)).astype(BF16)
     send_grad = (dot("ect,td->ecd", table, out_grad_q) * slot_weight[:, :, None]).astype(BF16)
     slot_rows = experts * capacity
-    rows_q = lax.all_to_all(send_rows, "sp", split_axis=0, concat_axis=0, tiled=True)
-    grad_q = lax.all_to_all(send_grad, "sp", split_axis=0, concat_axis=0, tiled=True)
-    rows_in = join_features(rows_q.reshape(slot_rows, -1))
-    grad_in = join_features(grad_q.reshape(slot_rows, -1))
-
     span_sums = jnp.cumsum(log_decay, axis=1)
     spot = jnp.arange(tok_rows)
     lower = (spot[:, None] >= spot[None, :])[None]
@@ -111,8 +298,16 @@
         "htk,hkv->htv", query_heads, state
     )
     mixed_flat = mixed_heads.astype(BF16).transpose(1, 0, 2).reshape(tok_rows, -1)
+    totals = lax.all_gather(span_sums[:, -1], "sp", axis=0)
+
+    sent = jnp.concatenate([send_rows, send_grad], axis=2)
+    sent, mixed_flat, totals = lax.optimization_barrier((sent, mixed_flat, totals))
     mixed_all = lax.all_gather(mixed_flat, "sp", axis=0, tiled=True)
-    totals = lax.all_gather(span_sums[:, -1], "sp", axis=0)
+    arrived = dispatch(sent)
+    arrived = arrived.reshape(arrived.shape[0], slot_rows, -1)
+    share = send_rows.shape[2]
+    rows_in = jnp.concatenate([block[:, :share] for block in arrived], axis=1)
+    grad_in = jnp.concatenate([block[:, share:] for block in arrived], axis=1)
 
     gate_pre = dot("rd,df->rf", rows_in, wg)
     up_pre = dot("rd,df->rf", rows_in, wu)
@@ -122,14 +317,14 @@
     gate_back = (hidden_back * up_pre * silu_slope(gate_pre)).astype(BF16)
     up_back = (hidden_back * active).astype(BF16)
     partial_value = dot("rf,df->rd", gate_back, wg) + dot("rf,df->rd", up_back, wu)
-    part = sum_features(partial_value.astype(BF16))
+    partial_value = partial_value.astype(BF16).reshape(experts, capacity, model_width)
+    parts = jnp.stack(jnp.split(partial_value, model_width // share, axis=2))
     down_grad = dot("rf,rd->fd", hidden, grad_in).astype(BF16)
     gate_grad = dot("rd,rf->df", rows_in, gate_back).astype(BF16)
     up_grad = dot("rd,rf->df", rows_in, up_back).astype(BF16)
 
-    returned = lax.all_to_all(
-        part.reshape(experts, capacity, -1), "sp", split_axis=0, concat_axis=0, tiled=True
-    )
+    parts, mixed_all = lax.optimization_barrier((parts, mixed_all))
+    returned = combine(parts)
     mixed_q = (out_grad_q.astype(F32) + dot("ect,ecd->td", table, returned)).astype(BF16)
     mixed_grad = lax.all_gather(mixed_q, "tp", axis=1, tiled=True)
 
@@ -145,13 +340,8 @@
     weight = jnp.where((later > place)[:, None], jnp.exp(between_sum), 0.0)
     incoming = jnp.sum(carried_all.astype(F32) * weight[:, :, None, None], axis=0).astype(BF16)
 
-    mixed_cols = lax.all_to_all(
-        mixed_grad.reshape(tok_rows, spans, -1).transpose(1, 0, 2),
-        "sp",
-        split_axis=0,
-        concat_axis=0,
-        tiled=True,
-    ).reshape(spans * tok_rows, -1)
+    mixed_cols = swap(mixed_grad.reshape(tok_rows, spans, -1).transpose(1, 0, 2))
+    mixed_cols = mixed_cols.reshape(spans * tok_rows, -1)
     out_proj_grad = dot("td,tc->dc", mixed_cols, mixed_all)
 
     back_scores = (dot("htv,hsv->hts", head_grad, value_heads) * (decay * scale)).astype(BF16)

time: 196 us -> 195 us (level)
  Pallas kernels: 0 us -> 65.6 us
  blocking collectives: 82.5 us -> 30.3 us
  waiting for transfers between devices: 43.3 us -> 32.5 us
  starting transfers between devices: 4.31 us -> 0.08 us
    pallas_call x0 -> x3, Pallas kernels: none -> 65.6 us  [the longest x1 27.6 us: dispatch(): pl.pallas_call(dispatch_kernel, out_shape=jax.ShapeDtypeStruct((members,)...]
    all_to_all x3 -> x0, blocking collectives: 56.1 us -> none  [the longest x1 24.2 us: body(): lax.all_to_all(part.reshape(experts, capacity, -1), 'sp', split_axis=0, c...]
    all_gather x1, waiting for transfers between devices: 0.02 us -> 18.7 us  [body(): lax.all_gather(carried.reshape(1, -1, value_size), 'sp', axis=0, tiled=True)]
    all_to_all x1 -> x0, waiting for transfers between devices: 18.2 us -> none  [body(): lax.all_to_all(mixed_grad.reshape(tok_rows, spans, -1).transpose(1, 0, 2)...]
    all_gather x1, waiting for transfers between devices: 0.01 us -> 13.8 us  [body(): mixed_all = lax.all_gather(mixed_flat, 'sp', axis=0, tiled=True)]
    all_gather x2 -> x0, waiting for transfers between devices: 13.3 us -> none  [join_features(): gathered = lax.all_gather(rows, 'tp', axis=0)]
    ppermute x2 -> x0, waiting for transfers between devices: 11.7 us -> none  [exchange(): return lax.ppermute(array, axis, [(i, i ^ step) for i in range(count)])]
    all_to_all x1 -> x0, starting transfers between devices: 3.5 us -> none  [body(): lax.all_to_all(mixed_grad.reshape(tok_rows, spans, -1).transpose(1, 0, 2)...]
  transfers between devices with their start and end apart: 7 -> 2, of which waited for: 4 -> 2; matrix products, arithmetic and copies ran while one was open for 21% -> 13% of each run, Pallas kernels for 0% -> 24%
where the time goes in v2:
time: 195 us; the launch traced here: 194 us
  Pallas kernels  65.6 us (34%)
  matrix products  32.8 us (17%)
  waiting for transfers between devices  32.5 us (17%)
  blocking collectives  30.3 us (16%)
  between operations  15.3 us (8%)
  local copies, waits for them, and re-layouts  9.64 us (5%)
  other arithmetic  7.59 us (4%)
    dot_general x24, matrix products, dot(): return jnp.einsum(spec, a, b, preferred_element_type=F32)  29.8 us
    pallas_call x1, Pallas kernels, dispatch(): pl.pallas_call(dispatch_kernel, out_shape=jax.ShapeDtypeStruct((members,)...  27.6 us
    unnamed x1, blocking collectives  23.1 us
    pallas_call x1, Pallas kernels, combine(): pl.pallas_call(combine_kernel, out_shape=jax.ShapeDtypeStruct((spans, row...  19.3 us
    pallas_call x1, Pallas kernels, swap(): pl.pallas_call(swap_kernel, out_shape=jax.ShapeDtypeStruct(blocks.shape,...  18.8 us
    all_gather x1, waiting for transfers between devices, body(): lax.all_gather(carried.reshape(1, -1, value_size), 'sp', axis=0, tiled=True)  18.7 us
    all_gather x1, waiting for transfers between devices, body(): mixed_all = lax.all_gather(mixed_flat, 'sp', axis=0, tiled=True)  13.8 us
    all_gather x1, blocking collectives, body(): mixed_grad = lax.all_gather(mixed_q, 'tp', axis=1, tiled=True)  7.18 us
  transfers between devices with their start and end apart: 2, of which 2 were waited for; matrix products, arithmetic and copies ran while one was open for 13% of the time, Pallas kernels for 24%

profile of v2, /device:TPU:0, one launch (start us, length us, event | category | flops | bytes accessed | tf_op | source)
XLA Modules:
  0.0 193.9 jit_solution(17707214407610798622)
XLA Ops:
  7.3 0.8 fusion.55
  8.3 0.7 select_reduce_fusion.2
  9.0 1.0 reduce_window_sum.11
  10.0 0.2 slice_reduce_fusion
  10.2 0.7 exponential_multiply_fusion
  10.8 1.3 fusion.14
  12.2 1.2 fusion.25
  13.4 0.6 copy-done.10
  14.0 0.2 fusion.19
  14.3 0.8 copy.53
  15.1 0.6 dynamic-slice
  16.4 0.2 dynamic-update-slice
  16.6 23.1 %all-reduce = f32[32]{0:T(128)S(1)} all-reduce(f32[32]{0:T(128)S(1)} %dynamic-update-slice), channel_id=2, replica_groups=mesh['sp'=8,'tp'=4] {'sp'}, use_global_device_ids=true, to_apply=%add | all-reduce | flops 32 | bytes 256
  39.9 1.1 convolution_convert_fusion.3
  41.1 1.2 fusion.17
  42.2 0.9 pad_maximum_fusion.3.x
  43.2 27.6 %shard_map.180 = bf16[4,8,40,1024]{3,2,1,0:T(8,128)(2,1)} custom-call(bf16[8,40,1024]{2,1,0:T(8,128)(2,1)} %pad_maximum_fusion.3.x), custom_call_target="tpu_custom_call" | custom-call | bytes 62914560 | tf_op jit(solution)/shard_map/pallas_call | solution.py:118
  70.8 1.9 %fusion.62 = (bf16[1,8,40,1024]{3,2,1,0:T(8,128)(2,1)S(1)}, bf16[1,8,40,1024]{3,2,1,0:T(8,128)(2,1)S(1)}, bf16[1,8,40,1024]{3,2,1,0:T(8,128)(2,1)S(1)}, bf16[1,8,40,1024]{3,2,1,0:T(8,128)(2,1)S(1)}) fusion(bf16[4,8,40,1024]{3,2,1,0:T(8,128)(2,1)} %shard_map.180), kind=kLoop, calls=%fused_computation.105 | loop fusion | bytes 5242880 | tf_op jit(solution)/shard_map/unstack | solution.py:309
  73.1 2.3 %copy-done.1 = bf16[1,2048,512]{2,1,0:T(8,128)(2,1)S(1)} copy-done((bf16[1,2048,512]{2,1,0:T(8,128)(2,1)S(1)}, bf16[1,2048,512]{2,1,0:T(8,128)(2,1)}, u32[]{:S(2)}) %copy-start.1) | copy-done | bytes 2097176
  75.4 0.8 fusion.9
  76.3 0.8 fusion.6
  77.2 0.9 copy-done.34
  78.1 1.1 multiply_convert_fusion.1
  79.2 0.9 fusion.4
  80.1 0.9 fusion.3
  81.1 1.2 pad_maximum_fusion.2.x
  82.3 13.8 %all-gather.4.cloned.1.call-done = bf16[1024,1024]{0,1:T(8,128)(2,1)} async-done(((bf16[128,1024]{0,1:T(8,128)(2,1)}), bf16[1024,1024]{0,1:T(8,128)(2,1)}) %all-gather.4.cloned.1.call-update) | async-done | bytes 2097168 | tf_op jit(solution)/shard_map/all_gather | solution.py:305
  96.1 19.3 %shard_map.181 = bf16[8,40,512]{2,1,0:T(8,128)(2,1)} custom-call(bf16[4,8,40,512]{3,2,1,0:T(8,128)(2,1)} %pad_maximum_fusion.2.x), custom_call_target="tpu_custom_call" | custom-call | bytes 47185920 | tf_op jit(solution)/shard_map/pallas_call | solution.py:238
  115.4 1.3 fusion.24
  116.7 7.2 %all_gather.14 = bf16[128,2048]{1,0:T(8,128)(2,1)S(1)} all-gather(bf16[128,512]{1,0:T(8,128)(2,1)S(1)} %fusion.24), channel_id=1, replica_groups=mesh['sp'=8,'tp'=4] {'tp'}, dimensions={1}, use_global_device_ids=true | all-gather | bytes 655360 | tf_op jit(solution)/shard_map/all_gather | solution.py:329
  123.9 2.9 %convolution_convert_fusion.5 = bf16[128,1024]{1,0:T(8,128)(2,1)S(1)} fusion(bf16[128,2048]{1,0:T(8,128)(2,1)S(1)} %all_gather.14, bf16[2048,1024]{1,0:T(8,128)(2,1)} %param.20), kind=kOutput, calls=%fused_computation.34 | convolution fusion | flops 537001984 | bytes 4980736 | tf_op jit(solution)/shard_map/dot_general | solution.py:331
  126.8 1.1 convolution_convert_fusion.4
  128.2 4.1 %fusion.1 = bf16[1,2048,512]{2,1,0:T(8,128)(2,1)} fusion(bf16[320,512]{1,0:T(8,128)(2,1)} %copy-done.13, bf16[320,512]{1,0:T(8,128)(2,1)} %copy-done.28, bf16[320,512]{1,0:T(8,128)(2,1)} %copy-done.26, bf16[320,512]{1,0:T(8,128)(2,1)} %copy-done.20, bf16[320,512]{1,0:T(8,128)(2,1)} %copy-done.18), kind=kOutput, calls=%fused_computation.6 | convolution fusion | flops 677380096 | bytes 3735552 | tf_op jit(solution)/shard_map/rd,rf->df/dot_general | solution.py:13
  132.4 2.6 %fusion = bf16[1,2048,512]{2,1,0:T(8,128)(2,1)} fusion(bf16[320,512]{1,0:T(8,128)(2,1)S(1)} %get-tuple-element.26, bf16[320,512]{1,0:T(8,128)(2,1)S(1)} %copy-done.29, bf16[320,512]{1,0:T(8,128)(2,1)S(1)} %copy-done.27, bf16[320,512]{1,0:T(8,128)(2,1)S(1)} %copy-done.21, bf16[320,512]{1,0:T(8,128)(2,1)S(1)} %copy-done.19), kind=kOutput, calls=%fused_computation.5 | convolution fusion | flops 677380096 | bytes 3735552 | tf_op jit(solution)/shard_map/rd,rf->df/dot_general | solution.py:13
  135.0 2.6 %fusion.2 = bf16[1,512,2048]{2,1,0:T(8,128)(2,1)} fusion(f32[320,512]{1,0:T(8,128)S(1)} %copy-done.37, bf16[320,512]{1,0:T(8,128)(2,1)S(1)} %copy-done.25, bf16[320,512]{1,0:T(8,128)(2,1)S(1)} %copy-done.23, bf16[320,512]{1,0:T(8,128)(2,1)S(1)} %copy-done.17, bf16[320,512]{1,0:T(8,128)(2,1)S(1)} %copy-done.15, f32[320,512]{1,0:T(8,128)S(1)} %copy-done.39), kind=kOutput, calls=%fused_computation.7 | convolution fusion | flops 678363136 | bytes 4718592 | tf_op jit(solution)/shard_map/rf,rd->fd/dot_general | solution.py:13
  137.7 0.3 copy.54
  137.9 1.0 copy.55
  139.0 18.8 %shard_map.182 = bf16[8,128,256]{2,1,0:T(8,128)(2,1)} custom-call(bf16[8,128,256]{2,1,0:T(8,128)(2,1)} %bitcast.137), custom_call_target="tpu_custom_call" | custom-call | bytes 31457280 | tf_op jit(solution)/shard_map/pallas_call | solution.py:150
  157.8 1.1 fusion.26
  158.9 0.9 fusion.69
  159.8 0.2 fusion.68
  160.0 1.2 fusion.30
  161.2 1.6 fusion.27
  162.8 1.7 fusion.67
  164.5 18.7 %all-gather.6.cloned.1.call-done = bf16[8,512,256]{2,1,0:T(8,128)(2,1)} async-done(((bf16[1,512,256]{2,1,0:T(8,128)(2,1)}), bf16[8,512,256]{2,1,0:T(8,128)(2,1)}) %all-gather.6.cloned.1.call-update) | async-done | bytes 2097168 | tf_op jit(solution)/shard_map/all_gather | solution.py:335
  183.2 2.0 %multiply_reduce_fusion = bf16[512,256]{1,0:T(8,128)(2,1)S(1)} fusion(bf16[8,512,256]{2,1,0:T(8,128)(2,1)} %all-gather.6.cloned.1.call-done, f32[8,512]{1,0:T(8,128)S(1)} %broadcast_bitcast_fusion), kind=kLoop, calls=%fused_computation | loop fusion | flops 3014656 | bytes 2375680 | tf_op jit(solution)/shard_map/reduce_sum | solution.py:341
  185.2 0.9 fusion.18
  186.1 0.9 fusion.28
  (95 shorter events, 1.2 us)
Async XLA Ops:
  7.2 69.1 %copy-start = (bf16[1,2048,512]{2,1,0:T(8,128)(2,1)S(1)}, bf16[1,2048,512]{2,1,0:T(8,128)(2,1)}, u32[]{:S(2)}) copy-start(bf16[1,2048,512]{2,1,0:T(8,128)(2,1)} %param.17) | copy-start | bytes 6291460
  7.2 7.9 %copy-start.35 = (u32[32]{0:T(128)S(1)}, u32[32]{0:T(128)}, u32[]{:S(2)}) copy-start(u32[32]{0:T(128)} %constant.35) | copy-start | bytes 388
  7.2 6.8 %copy-start.7 = (bf16[4,128,256]{2,1,0:T(8,128)(2,1)S(1)}, bf16[4,128,256]{2,1,0:T(8,128)(2,1)}, u32[]{:S(2)}) copy-start(bf16[4,128,256]{2,1,0:T(8,128)(2,1)} %param.23) | copy-start | bytes 786436
  7.2 88.9 %all-gather.4.cloned.1.call-start = ((), (), s32[]{:S(2)}) async-start(), calls=%async_computation | async-start | bytes 2359296 | tf_op jit(solution)/shard_map/all_gather | solution.py:305
  7.3 4.9 %copy-start.33 = (pred[128,128]{1,0:T(8,128)(4,1)}, pred[128,128]{1,0:T(8,128)(4,1)S(1)}, u32[]{:S(2)}) copy-start(pred[128,128]{1,0:T(8,128)(4,1)S(1)} %iota_compare_fusion.1) | copy-start | bytes 49156
  10.0 2.2 %copy-start.32 = (f32[4,128]{1,0:T(4,128)}, f32[4,128]{1,0:T(4,128)S(1)}, u32[]{:S(2)}) copy-start(f32[4,128]{1,0:T(4,128)S(1)} %reduce_window_sum.11) | copy-start | bytes 6148
  10.8 116.0 %copy-start.31 = (f32[4,128]{1,0:T(4,128)}, f32[4,128]{1,0:T(4,128)S(1)}, u32[]{:S(2)}) copy-start(f32[4,128]{1,0:T(4,128)S(1)} %get-tuple-element.37) | copy-start | bytes 6148
  13.4 0.7 copy-start.10
  43.2 140.0 %all-gather.6.cloned.1.call-start = ((), (), s32[]{:S(2)}) async-start(), calls=%async_computation.1 | async-start | bytes 2359296 | tf_op jit(solution)/shard_map/all_gather | solution.py:335
  72.8 2.6 %copy-start.1 = (bf16[1,2048,512]{2,1,0:T(8,128)(2,1)S(1)}, bf16[1,2048,512]{2,1,0:T(8,128)(2,1)}, u32[]{:S(2)}) copy-start(bf16[1,2048,512]{2,1,0:T(8,128)(2,1)} %param.18) | copy-start | bytes 6291460
  72.9 3.3 %copy-start.18 = (bf16[320,512]{1,0:T(8,128)(2,1)}, bf16[320,512]{1,0:T(8,128)(2,1)S(1)}, u32[]{:S(2)}) copy-start(bf16[320,512]{1,0:T(8,128)(2,1)S(1)} %get-tuple-element.28) | copy-start | bytes 983044
  72.9 3.3 %copy-start.20 = (bf16[320,512]{1,0:T(8,128)(2,1)}, bf16[320,512]{1,0:T(8,128)(2,1)S(1)}, u32[]{:S(2)}) copy-start(bf16[320,512]{1,0:T(8,128)(2,1)S(1)} %get-tuple-element.38) | copy-start | bytes 983044
  72.9 4.2 %copy-start.14 = (bf16[320,512]{1,0:T(8,128)(2,1)}, bf16[320,512]{1,0:T(8,128)(2,1)S(1)}, u32[]{:S(2)}) copy-start(bf16[320,512]{1,0:T(8,128)(2,1)S(1)} %get-tuple-element.27) | copy-start | bytes 983044
  72.9 4.2 %copy-start.16 = (bf16[320,512]{1,0:T(8,128)(2,1)}, bf16[320,512]{1,0:T(8,128)(2,1)S(1)}, u32[]{:S(2)}) copy-start(bf16[320,512]{1,0:T(8,128)(2,1)S(1)} %get-tuple-element.39) | copy-start | bytes 983044
  73.1 3.2 %copy-start.26 = (bf16[320,512]{1,0:T(8,128)(2,1)}, bf16[320,512]{1,0:T(8,128)(2,1)S(1)}, u32[]{:S(2)}) copy-start(bf16[320,512]{1,0:T(8,128)(2,1)S(1)} %get-tuple-element.32) | copy-start | bytes 983044
  73.1 3.2 %copy-start.28 = (bf16[320,512]{1,0:T(8,128)(2,1)}, bf16[320,512]{1,0:T(8,128)(2,1)S(1)}, u32[]{:S(2)}) copy-start(bf16[320,512]{1,0:T(8,128)(2,1)S(1)} %get-tuple-element.40) | copy-start | bytes 983044
  73.1 4.1 %copy-start.22 = (bf16[320,512]{1,0:T(8,128)(2,1)}, bf16[320,512]{1,0:T(8,128)(2,1)S(1)}, u32[]{:S(2)}) copy-start(bf16[320,512]{1,0:T(8,128)(2,1)S(1)} %get-tuple-element.31) | copy-start | bytes 983044
  73.1 4.1 %copy-start.24 = (bf16[320,512]{1,0:T(8,128)(2,1)}, bf16[320,512]{1,0:T(8,128)(2,1)S(1)}, u32[]{:S(2)}) copy-start(bf16[320,512]{1,0:T(8,128)(2,1)S(1)} %get-tuple-element.41) | copy-start | bytes 983044
  76.3 0.9 copy-start.36
  76.3 1.8 copy-start.34
  77.1 2.0 %copy-start.38 = (f32[320,512]{1,0:T(8,128)}, f32[320,512]{1,0:T(8,128)S(1)}, u32[]{:S(2)}) copy-start(f32[320,512]{1,0:T(8,128)S(1)} %fusion.6) | copy-start | bytes 1966084
  79.2 0.9 copy-start.13
  123.9 3.0 %copy-start.5 = (bf16[4,128,128]{2,1,0:T(8,128)(2,1)S(1)}, bf16[4,128,128]{2,1,0:T(8,128)(2,1)}, u32[]{:S(2)}) copy-start(bf16[4,128,128]{2,1,0:T(8,128)(2,1)} %param.21) | copy-start | bytes 393220
  128.2 4.1 %copy-start.19 = (bf16[320,512]{1,0:T(8,128)(2,1)S(1)}, bf16[320,512]{1,0:T(8,128)(2,1)}, u32[]{:S(2)}) copy-start(bf16[320,512]{1,0:T(8,128)(2,1)} %copy-done.18) | copy-start | bytes 983044
  128.2 4.1 %copy-start.21 = (bf16[320,512]{1,0:T(8,128)(2,1)S(1)}, bf16[320,512]{1,0:T(8,128)(2,1)}, u32[]{:S(2)}) copy-start(bf16[320,512]{1,0:T(8,128)(2,1)} %copy-done.20) | copy-start | bytes 983044
  128.2 4.1 %copy-start.27 = (bf16[320,512]{1,0:T(8,128)(2,1)S(1)}, bf16[320,512]{1,0:T(8,128)(2,1)}, u32[]{:S(2)}) copy-start(bf16[320,512]{1,0:T(8,128)(2,1)} %copy-done.26) | copy-start | bytes 983044
  128.2 4.1 %copy-start.29 = (bf16[320,512]{1,0:T(8,128)(2,1)S(1)}, bf16[320,512]{1,0:T(8,128)(2,1)}, u32[]{:S(2)}) copy-start(bf16[320,512]{1,0:T(8,128)(2,1)} %copy-done.28) | copy-start | bytes 983044
  132.3 2.7 %copy-start.15 = (bf16[320,512]{1,0:T(8,128)(2,1)S(1)}, bf16[320,512]{1,0:T(8,128)(2,1)}, u32[]{:S(2)}) copy-start(bf16[320,512]{1,0:T(8,128)(2,1)} %copy-done.14) | copy-start | bytes 983044
  132.3 2.7 %copy-start.17 = (bf16[320,512]{1,0:T(8,128)(2,1)S(1)}, bf16[320,512]{1,0:T(8,128)(2,1)}, u32[]{:S(2)}) copy-start(bf16[320,512]{1,0:T(8,128)(2,1)} %copy-done.16) | copy-start | bytes 983044
  132.3 2.7 %copy-start.23 = (bf16[320,512]{1,0:T(8,128)(2,1)S(1)}, bf16[320,512]{1,0:T(8,128)(2,1)}, u32[]{:S(2)}) copy-start(bf16[320,512]{1,0:T(8,128)(2,1)} %copy-done.22) | copy-start | bytes 983044
  132.3 2.6 %copy-start.25 = (bf16[320,512]{1,0:T(8,128)(2,1)S(1)}, bf16[320,512]{1,0:T(8,128)(2,1)}, u32[]{:S(2)}) copy-start(bf16[320,512]{1,0:T(8,128)(2,1)} %copy-done.24) | copy-start | bytes 983044
  132.3 2.6 %copy-start.37 = (f32[320,512]{1,0:T(8,128)S(1)}, f32[320,512]{1,0:T(8,128)}, u32[]{:S(2)}) copy-start(f32[320,512]{1,0:T(8,128)} %copy-done.36) | copy-start | bytes 1966084
  132.4 2.6 %copy-start.39 = (f32[320,512]{1,0:T(8,128)S(1)}, f32[320,512]{1,0:T(8,128)}, u32[]{:S(2)}) copy-start(f32[320,512]{1,0:T(8,128)} %copy-done.38) | copy-start | bytes 1966084
  137.9 19.8 %copy-start.8 = (bf16[4,128,256]{2,1,0:T(8,128)(2,1)S(1)}, bf16[4,128,256]{2,1,0:T(8,128)(2,1)}, u32[]{:S(2)}) copy-start(bf16[4,128,256]{2,1,0:T(8,128)(2,1)} %param.23) | copy-start | bytes 786436
  137.9 21.9 %copy-start.11 = (bf16[4,128,128]{2,1,0:T(8,128)(2,1)S(1)}, bf16[4,128,128]{2,1,0:T(8,128)(2,1)}, u32[]{:S(2)}) copy-start(bf16[4,128,128]{2,1,0:T(8,128)(2,1)} %param.22) | copy-start | bytes 393220
  139.0 22.2 %copy-start.4 = (f32[4,1,128,256]{3,2,1,0:T(8,128)S(1)}, f32[4,1,128,256]{3,2,1,0:T(8,128)}, u32[]{:S(2)}) copy-start(f32[4,1,128,256]{3,2,1,0:T(8,128)} %param.25) | copy-start | bytes 1572868
  157.7 5.0 %copy-start.2 = (bf16[1024,1024]{0,1:T(8,128)(2,1)S(1)}, bf16[1024,1024]{0,1:T(8,128)(2,1)}, u32[]{:S(2)}) copy-start(bf16[1024,1024]{0,1:T(8,128)(2,1)} %all-gather.4.cloned.1.call-done) | copy-start | bytes 6291460
  157.7 5.0 %copy-start.3 = (bf16[8,128,256]{2,1,0:T(8,128)(2,1)S(1)}, bf16[8,128,256]{2,1,0:T(8,128)(2,1)}, u32[]{:S(2)}) copy-start(bf16[8,128,256]{2,1,0:T(8,128)(2,1)} %shard_map.182) | copy-start | bytes 1572868
  164.5 20.7 %copy-start.12 = (bf16[4,128,128]{2,1,0:T(8,128)(2,1)S(1)}, bf16[4,128,128]{2,1,0:T(8,128)(2,1)}, u32[]{:S(2)}) copy-start(bf16[4,128,128]{2,1,0:T(8,128)(2,1)} %param.22) | copy-start | bytes 393220
  164.5 20.7 %copy-start.30 = (f32[4,128]{1,0:T(4,128)S(1)}, f32[4,128]{1,0:T(4,128)}, u32[]{:S(2)}) copy-start(f32[4,128]{1,0:T(4,128)} %get-tuple-element.35) | copy-start | bytes 6148
  164.5 21.6 %copy-start.6 = (f32[4,128,128]{2,1,0:T(8,128)S(1)}, f32[4,128,128]{2,1,0:T(8,128)}, u32[]{:S(2)}) copy-start(f32[4,128,128]{2,1,0:T(8,128)} %fusion.69) | copy-start | bytes 786436
  164.5 21.6 %copy-start.9 = (bf16[4,128,256]{2,1,0:T(8,128)(2,1)S(1)}, bf16[4,128,256]{2,1,0:T(8,128)(2,1)}, u32[]{:S(2)}) copy-start(bf16[4,128,256]{2,1,0:T(8,128)(2,1)} %param.23) | copy-start | bytes 786436
Sparse Core Ops, SparseCore 0:
  43.3 52.7 all-gather.3
  128.0 55.0 all-gather.5
